TPU v7x, 512 devices: a whole 4x4x16 slice. The times are simulated.
512 devices in a mesh: ep: 32 (over z, core), tp: 16 (over y, x).
Axes of the slice: x: 4, y: 4, z: 16, core: 2. Of those that a mesh axis runs over, the one named last changes fastest.
Arguments:
- conv_input: bfloat16 [1024, 65536], P('tp', 'ep'), may hold values from -6 to 6
- out_gate: bfloat16 [1024, 65536], P('tp', 'ep'), may hold values from -6 to 6
- in_gate: bfloat16 [1024, 65536], P('tp', 'ep'), may hold values from -6 to 6
- conv_taps: float32 [3, 1024], replicated, may hold values from -3.5 to 3.5
- mixer_proj: bfloat16 [1024, 2048], P(None, 'tp'), may hold values from -0.1875 to 0.1875
- token_rows: bfloat16 [8192, 2048], P('ep', 'tp'), may hold values from -4000 to 4000
- routes: int32 [8192, 2], P('ep'), may hold values from 0 to 31, as said below
- route_weights: float32 [8192, 2], P('ep'), may hold values from 0.3 to 1
- expert_gate: bfloat16 [32, 2048, 4096], P('ep', None, 'tp'), may hold values from -0.125 to 0.125
- expert_up: bfloat16 [32, 2048, 4096], P('ep', None, 'tp'), may hold values from -0.125 to 0.125
- expert_down: bfloat16 [32, 4096, 2048], P('ep', 'tp'), may hold values from -0.125 to 0.125
Outputs:
- mixed_out: bfloat16 [65536, 2048], P('ep', 'tp')
- expert_out: bfloat16 [8192, 2048], P('ep', 'tp')
Inputs may be any that keep to these rules, and one draw needn't show every extreme that they name: `routes`: in each aligned block of 256 rows, no expert is named more than 32 times and one expert, the same in every block, exactly 32 times; the two experts of a row differ.
All inputs are finite; a program needn't handle non-finite values.
Results may differ from a plain program's by a relative error of at most 0.015.
Values may be sent and summed in bfloat16 or wider, within the bound.
No kernel may reach another device: no remote copies, remote signals or barrier semaphores. Data moves between devices by JAX's collectives and lax.ppermute only.
A program may use at most 64 MiB of HBM per device.

v0:
```python
import functools

import jax
import jax.numpy as jnp
from jax import lax
from jax.experimental import pallas as pl
from jax.experimental.pallas import tpu as pltpu
from jax.sharding import Mesh
from jax.sharding import PartitionSpec as P

KERNEL = 3
EPSILON = 1e-06
BF = jnp.bfloat16
F32 = jnp.float32


def ones_where(test):
    return jnp.where(test, 1.0, 0.0).astype(BF)


def dispatch_kernel(me_ref, routes_ref, rows_ref, places_ref, out_ref, *, experts, tp):
    core = me_ref[0] // tp
    rows = rows_ref.shape[0]
    slot_total = out_ref.shape[0]
    capacity = slot_total // experts
    ids = lax.broadcasted_iota(jnp.int32, (experts, rows), 0)
    named = [routes_ref[k : k + 1, :] for k in range(2)]
    hit = [n == ids for n in named]
    sooner = lax.broadcasted_iota(jnp.int32, (rows, rows), 0)
    later = lax.broadcasted_iota(jnp.int32, (rows, rows), 1)
    earlier = jnp.dot(
        ones_where(hit[0] | hit[1]), ones_where(sooner < later), preferred_element_type=F32
    )
    slots = lax.broadcasted_iota(jnp.int32, (slot_total, rows), 0)
    taken = []
    for k in range(2):
        slot = jnp.sum(jnp.where(hit[k], earlier, 0.0), axis=0, keepdims=True)
        place = (named[k] ^ core) * capacity + slot.astype(jnp.int32)
        places_ref[k : k + 1, :] = place
        taken.append(place == slots)
    out_ref[...] = jnp.dot(
        ones_where(taken[0] | taken[1]), rows_ref[...], preferred_element_type=F32
    ).astype(BF)


def combine_kernel(places_ref, weights_ref, own_ref, other_ref, out_ref, *, capacity):
    rows = out_ref.shape[0]
    slots = lax.broadcasted_iota(jnp.int32, (own_ref.shape[0], rows), 0)
    total = None
    for k in range(2):
        place = places_ref[k : k + 1, :]
        group = place // capacity
        within = (group // 2) * capacity + place % capacity
        match = within == slots
        picked = None
        for side, ref in enumerate((own_ref, other_ref)):
            part = lax.dot_general(
                ones_where(match & (group % 2 == side)),
                ref[...],
                (((0,), (0,)), ((), ())),
                preferred_element_type=F32,
            )
            picked = part if picked is None else picked + part
        term = picked * weights_ref[:, k : k + 1]
        total = term if total is None else total + term
    out_ref[...] = total.astype(BF)


def sum_kernel(in_ref, out_ref):
    total = in_ref[0].astype(F32)
    for j in range(1, in_ref.shape[0]):
        total = total + in_ref[j].astype(F32)
    out_ref[...] = total.astype(BF)


def expert_kernel(me_ref, x_ref, gate_ref, up_ref, down_ref, out_ref):
    parts = x_ref.shape[0]
    cols = x_ref.shape[2]
    side = 4
    core = me_ref[0] // parts
    natural = [j for j in range(parts)]
    turned = [(j % side) * side + j // side for j in range(parts)]
    load = [jnp.where(core == 0, natural[j], turned[j]) for j in range(parts)]
    store = [jnp.where(core == 0, turned[j], natural[j]) for j in range(parts)]
    x = jnp.concatenate([x_ref[load[j]] for j in range(parts)], axis=1)
    values = x.astype(F32)
    squares = jnp.sum(values * values, axis=1, keepdims=True)
    scale = lax.rsqrt(squares / (parts * cols) + EPSILON)
    gate = scale * jnp.dot(x, gate_ref[...], preferred_element_type=F32)
    up = scale * jnp.dot(x, up_ref[...], preferred_element_type=F32)
    hidden = (jax.nn.silu(gate) * up).astype(BF)
    part = jnp.dot(hidden, down_ref[...], preferred_element_type=F32).astype(BF)
    for j in range(parts):
        out_ref[store[j]] = part[:, j * cols : (j + 1) * cols]


def expert_part(me, x, gate_weight, up_weight, down_weight, tile):
    parts, rows, cols = x.shape
    whole = lambda w: pl.BlockSpec(w.shape, lambda i, c: (0, 0))
    return pl.pallas_call(
        expert_kernel,
        grid_spec=pltpu.PrefetchScalarGridSpec(
            num_scalar_prefetch=1,
            grid=(rows // tile,),
            in_specs=[
                pl.BlockSpec((parts, tile, cols), lambda i, c: (0, i, 0)),
                whole(gate_weight),
                whole(up_weight),
                whole(down_weight),
            ],
            out_specs=pl.BlockSpec((parts, tile, cols), lambda i, c: (0, i, 0)),
        ),
        out_shape=jax.ShapeDtypeStruct(x.shape, BF),
        compiler_params=pltpu.CompilerParams(vmem_limit_bytes=28 * 1024 * 1024),
        cost_estimate=pl.CostEstimate(
            flops=6 * rows * parts * cols * gate_weight.shape[1],
            bytes_accessed=2 * 2 * rows * parts * cols + 6 * gate_weight.size,
            transcendentals=rows * gate_weight.shape[1],
        ),
    )(me.reshape(1), x, gate_weight, up_weight, down_weight)


def mixer_kernel(me_ref, *refs, fars, last):
    refs, out_ref = refs[:-1], refs[-1]
    proj_ref, refs = refs[0], refs[1:]
    blocks = proj_ref.shape[0]
    side = 4
    core = me_ref[0] // blocks
    row = (me_ref[0] % blocks) // side
    col = me_ref[0] % side
    weights = []
    for far in fars:
        for near in range(side):
            down = jnp.where(core == 0, far, near)
            right = jnp.where(core == 0, near, far)
            at = ((row + down) % side) * side + (col + right) % side
            weights.append(proj_ref[at])
    proj = jnp.concatenate(weights, axis=0)
    pieces = refs[:-1] if last else refs
    y = jnp.concatenate([ref[i] for ref in pieces for i in range(ref.shape[0])], axis=0)
    flat = lax.dot_general(
        proj, y, (((0,), (0,)), ((), ())), preferred_element_type=F32
    )
    if last:
        out_ref[...] = jnp.transpose(flat + refs[-1][...]).astype(BF)
    else:
        out_ref[...] = flat


def mixer_product(me, proj, pieces, fars, base, tile):
    length = pieces[0].shape[2]
    _, width, cols = proj.shape
    last = base is not None
    flat_spec = pl.BlockSpec((cols, tile), lambda i, c: (0, i))
    return pl.pallas_call(
        functools.partial(mixer_kernel, fars=fars, last=last),
        grid_spec=pltpu.PrefetchScalarGridSpec(
            num_scalar_prefetch=1,
            grid=(length // tile,),
            in_specs=[pl.BlockSpec(proj.shape, lambda i, c: (0, 0, 0))]
            + [
                pl.BlockSpec(p.shape[:2] + (tile,), lambda i, c: (0, 0, i)) for p in pieces
            ]
            + ([flat_spec] if last else []),
            out_specs=pl.BlockSpec((tile, cols), lambda i, c: (i, 0)) if last else flat_spec,
        ),
        out_shape=jax.ShapeDtypeStruct((length, cols), BF)
        if last
        else jax.ShapeDtypeStruct((cols, length), F32),
        compiler_params=pltpu.CompilerParams(vmem_limit_bytes=16 * 1024 * 1024),
        cost_estimate=pl.CostEstimate(
            flops=2 * length * len(fars) * 4 * width * cols,
            bytes_accessed=2 * length * (len(fars) * 4 * width + 2 * cols) + 2 * proj.size,
            transcendentals=0,
        ),
    )(me.reshape(1), proj, *pieces, *([base] if last else []))


def sum_parts(arrived, steps):
    parts, rows, cols = arrived.shape
    return pl.pallas_call(
        sum_kernel,
        grid=(steps,),
        in_specs=[pl.BlockSpec((parts, rows // steps, cols), lambda i: (0, i, 0))],
        out_specs=pl.BlockSpec((rows // steps, cols), lambda i: (i, 0)),
        out_shape=jax.ShapeDtypeStruct((rows, cols), BF),
        compiler_params=pltpu.CompilerParams(vmem_limit_bytes=12 * 1024 * 1024),
    )(arrived)


def layer(
    conv_input,
    out_gate,
    in_gate,
    conv_taps,
    mixer_proj,
    token_rows,
    routes,
    route_weights,
    expert_gate,
    expert_up,
    expert_down,
):
    depth = lax.axis_size("z")
    experts = 2 * depth
    tp = lax.axis_size("tp")
    me = lax.axis_index(("c", "tp"))
    rows_b, cols_part = token_rows.shape
    capacity = 4 * rows_b // experts
    slot_total = experts * capacity
    half = slot_total // 2

    by_choice = routes.T
    places, outgoing = pl.pallas_call(
        functools.partial(dispatch_kernel, experts=experts, tp=tp),
        grid_spec=pltpu.PrefetchScalarGridSpec(
            num_scalar_prefetch=1,
            grid=(1,),
            in_specs=[
                pl.BlockSpec(by_choice.shape, lambda i, c: (0, 0)),
                pl.BlockSpec(token_rows.shape, lambda i, c: (0, 0)),
            ],
            out_specs=[
                pl.BlockSpec(by_choice.shape, lambda i, c: (0, 0)),
                pl.BlockSpec((slot_total, cols_part), lambda i, c: (0, 0)),
            ],
        ),
        out_shape=[
            jax.ShapeDtypeStruct(by_choice.shape, jnp.int32),
            jax.ShapeDtypeStruct((slot_total, cols_part), BF),
        ],
        compiler_params=pltpu.CompilerParams(vmem_limit_bytes=12 * 1024 * 1024),
    )(me.reshape(1), by_choice, token_rows)
    outgoing, conv_input, in_gate = lax.optimization_barrier((outgoing, conv_input, in_gate))
    arrived = lax.all_to_all(
        outgoing.reshape(depth, 2, capacity, cols_part), "z", 0, 0, tiled=True
    )

    length = conv_input.shape[1]
    width_part = conv_input.shape[0]
    offset = lax.axis_index("tp") * width_part
    local_taps = lax.dynamic_slice_in_dim(conv_taps, offset, width_part, 1)
    z_rows = (conv_input.astype(F32) * in_gate.astype(F32)).astype(BF)
    pairs = [(i, i + 1) for i in range(experts - 1)]
    rim = lax.ppermute(z_rows[:, length - (KERNEL - 1) :], ("z", "c"), pairs)
    longer = jnp.concatenate([rim, z_rows], axis=1).astype(F32)
    conv_sum = jnp.zeros(z_rows.shape, F32)
    for lag in range(KERNEL):
        begin = KERNEL - 1 - lag
        conv_sum = conv_sum + local_taps[lag][:, None] * longer[:, begin : begin + length]
    gated = (out_gate.astype(F32) * conv_sum).astype(BF)
    side = 4
    swap = [(0, 1), (1, 0)]
    place = lambda c, y, x: (c * side + y) * side + x
    span = range(side)
    along_x = lambda c: [[place(c, y, x) for x in span] for y in span]
    along_y = lambda c: [[place(c, y, x) for y in span] for x in span]
    early = along_x(0) + along_y(1)
    late = along_y(0) + along_x(1)

    def step(value, by, phase):
        pairs = []
        for c in range(2):
            for y in span:
                for x in span:
                    if (c == 0) == (phase == 0):
                        to = place(c, y, (x + by) % side)
                    else:
                        to = place(c, (y + by) % side, x)
                    pairs.append((place(c, y, x), to))
        return lax.ppermute(value, ("c", "tp"), pairs)

    gated = gated.reshape(2, width_part // 2, length)
    before = step(gated, 1, 0)
    after = step(gated, -1, 0)
    far = step(gated, 2, 0)
    line = jnp.concatenate([gated, after, far, before], axis=0)

    def exchange(value, groups):
        return lax.all_to_all(
            value, ("c", "tp"), 0, 0, axis_index_groups=groups, tiled=True
        )

    rows_other = lax.ppermute(arrived[:, 1], "c", swap)
    rows = jnp.stack([arrived[:, 0], rows_other], axis=1).reshape(slot_total, cols_part)
    quarter = exchange(jnp.broadcast_to(rows[None], (side,) + rows.shape), early)
    quarter, line = lax.optimization_barrier((quarter, line))
    x = exchange(jnp.broadcast_to(quarter[None], (side,) + quarter.shape), late)
    x = x.reshape(tp, slot_total, cols_part)
    weights = (expert_gate[0], expert_up[0], expert_down[0])
    part = expert_part(me, x, *weights, rows_b)
    part = part.reshape(side, side, slot_total, cols_part)
    half_sums = exchange(part, early).reshape(side, side * slot_total, cols_part)
    half_sums = sum_parts(half_sums, 8).reshape(side, slot_total, cols_part)
    half_sums, line = lax.optimization_barrier((half_sums, line))
    line_before = step(line, 1, 1)
    line_after = step(line, -1, 1)
    line_far = step(line, 2, 1)
    expert_rows = exchange(half_sums, late)
    expert_rows = sum_parts(expert_rows, 2)
    back = expert_rows.reshape(depth, 2, capacity, cols_part)
    returned = lax.all_to_all(back, "z", 0, 0, tiled=True)
    blocks = mixer_proj.reshape(tp, width_part, cols_part)
    most = mixer_product(
        me, blocks, (line, line_after, line_before), (0, 1, 3), None, length // 4
    )
    returned, most = lax.optimization_barrier((returned, most))
    returned_own = returned[:, 0].reshape(half, cols_part)
    returned_other = lax.ppermute(returned[:, 1].reshape(half, cols_part), "c", swap)
    mixed_out = mixer_product(
        me, blocks, (line_far,), (2,), most, length // 4
    )
    returned_other, mixed_out = lax.optimization_barrier((returned_other, mixed_out))
    expert_out = pl.pallas_call(
        functools.partial(combine_kernel, capacity=capacity),
        out_shape=jax.ShapeDtypeStruct((rows_b, cols_part), BF),
        compiler_params=pltpu.CompilerParams(vmem_limit_bytes=12 * 1024 * 1024),
    )(places, route_weights, returned_own, returned_other)
    return (mixed_out, expert_out)


def solution(mesh):
    ep, tp = mesh.devices.shape
    fine = Mesh(mesh.devices.reshape(ep // 2, 2, tp), ("z", "c", "tp"))
    both = ("z", "c")
    return jax.shard_map(
        layer,
        mesh=fine,
        in_specs=(
            P("tp", both),
            P("tp", both),
            P("tp", both),
            P(),
            P(None, "tp"),
            P(both, "tp"),
            P(both, None),
            P(both, None),
            P(both, None, "tp"),
            P(both, None, "tp"),
            P(both, "tp", None),
        ),
        out_specs=(P(both, "tp"), P(both, "tp")),
        check_vma=False,
    )
```

profile of v0, /device:TPU:1, one launch (start us, length us, event | category | flops | bytes accessed | tf_op | source)
XLA Modules:
  0.0 183.3 jit_solution(16201105642543908660)
XLA Ops:
  4.0 15.7 %all-to-all-start = ((bf16[16,2,32,128]{3,2,1,0:T(8,128)(2,1)}), bf16[16,2,32,128]{3,2,1,0:T(8,128)(2,1)S(1)}, u32[]{:S(2)}, u32[]{:S(2)}) async-start(bf16[16,2,32,128]{3,2,1,0:T(8,128)(2,1)} %bitcast.2), calls=%async_computation | async-start | bytes 524288 | tf_op jit(solution)/shard_map/all_to_all | solution.py:235
  20.9 4.4 %collective-permute-start.1 = (bf16[64,2]{1,0:T(8,128)(2,1)S(1)}, bf16[64,2]{1,0:T(8,128)(2,1)S(1)}, u32[]{:S(2)}, u32[]{:S(2)}) collective-permute-start(bf16[64,2]{1,0:T(8,128)(2,1)S(1)} %slice.46), channel_id=1, source_target_pairs={{0,16},{16,32},{32,48},{48,64},{64,80},{80,96},{96,112},{112,128},... | collective-permute-start | bytes 776 | tf_op jit(solution)/shard_map/ppermute | solution.py:245
  25.4 8.1 %all-to-all-done = bf16[16,2,32,128]{3,2,1,0:T(8,128)(2,1)S(1)} async-done(((bf16[16,2,32,128]{3,2,1,0:T(8,128)(2,1)}), bf16[16,2,32,128]{3,2,1,0:T(8,128)(2,1)S(1)}, u32[]{:S(2)}, u32[]{:S(2)}) %all-to-all-start) | async-done | bytes 262176 | tf_op jit(solution)/shard_map/all_to_all | solution.py:235
  33.5 8.1 %collective-permute-start = (bf16[16,32,128]{2,1,0:T(8,128)(2,1)S(1)}, bf16[16,32,128]{2,1,0:T(8,128)(2,1)S(1)}, u32[]{:S(2)}, u32[]{:S(2)}) collective-permute-start(bf16[16,32,128]{2,1,0:T(8,128)(2,1)S(1)} %get-tuple-element.31), channel_id=1, source_target_pairs={{0,16},{16,0},{1,17},{17,1},{2,18},{18,2},{3,19},{19,3},{4,20},{20... | collective-permute-start | bytes 393224 | tf_op jit(solution)/shard_map/ppermute | solution.py:284
  43.8 4.2 %all-to-all-start.1 = ((bf16[4,1024,128]{2,1,0:T(8,128)(2,1)}), bf16[4,1024,128]{2,1,0:T(8,128)(2,1)S(1)}, u32[]{:S(2)}, u32[]{:S(2)}) async-start(bf16[4,1024,128]{2,1,0:T(8,128)(2,1)} %broadcast_in_dim.14), calls=%async_computation.1 | async-start | bytes 2097152 | tf_op jit(solution)/shard_map/all_to_all | solution.py:280
  48.3 4.6 %collective-permute-start.2 = (bf16[2,32,2048]{2,1,0:T(8,128)(2,1)S(1)}, bf16[2,32,2048]{2,1,0:T(8,128)(2,1)S(1)}, u32[]{:S(2)}, u32[]{:S(2)}) collective-permute-start(bf16[2,32,2048]{2,1,0:T(8,128)(2,1)S(1)} %bitcast.38), channel_id=1, source_target_pairs={{0,3},{1,0},{2,1},{3,2},{4,7},{5,4},{6,5},{7,6},{8,11},{9,8},{10,9... | collective-permute-start | bytes 786440 | tf_op jit(solution)/shard_map/ppermute | solution.py:271
  52.9 2.5 %collective-permute-start.3 = (bf16[2,32,2048]{2,1,0:T(8,128)(2,1)S(1)}, bf16[2,32,2048]{2,1,0:T(8,128)(2,1)S(1)}, u32[]{:S(2)}, u32[]{:S(2)}) collective-permute-start(bf16[2,32,2048]{2,1,0:T(8,128)(2,1)S(1)} %bitcast.39), channel_id=1, source_target_pairs={{0,2},{1,3},{2,0},{3,1},{4,6},{5,7},{6,4},{7,5},{8,10},{9,11},{10,... | collective-permute-start | bytes 786440 | tf_op jit(solution)/shard_map/ppermute | solution.py:271
  55.4 2.5 %collective-permute-start.4 = (bf16[2,32,2048]{2,1,0:T(8,128)(2,1)S(1)}, bf16[2,32,2048]{2,1,0:T(8,128)(2,1)S(1)}, u32[]{:S(2)}, u32[]{:S(2)}) collective-permute-start(bf16[2,32,2048]{2,1,0:T(8,128)(2,1)S(1)} %bitcast.40), channel_id=1, source_target_pairs={{0,1},{1,2},{2,3},{3,0},{4,5},{5,6},{6,7},{7,4},{8,9},{9,10},{10,1... | collective-permute-start | bytes 786440 | tf_op jit(solution)/shard_map/ppermute | solution.py:271
  59.3 2.5 %collective-permute-done.3 = bf16[2,32,2048]{2,1,0:T(8,128)(2,1)S(1)} collective-permute-done((bf16[2,32,2048]{2,1,0:T(8,128)(2,1)S(1)}, bf16[2,32,2048]{2,1,0:T(8,128)(2,1)S(1)}, u32[]{:S(2)}, u32[]{:S(2)}) %collective-permute-start.3) | collective-permute-done | bytes 262176 | tf_op jit(solution)/shard_map/ppermute | solution.py:271
  61.8 2.8 %collective-permute-done.4 = bf16[2,32,2048]{2,1,0:T(8,128)(2,1)S(1)} collective-permute-done((bf16[2,32,2048]{2,1,0:T(8,128)(2,1)S(1)}, bf16[2,32,2048]{2,1,0:T(8,128)(2,1)S(1)}, u32[]{:S(2)}, u32[]{:S(2)}) %collective-permute-start.4) | collective-permute-done | bytes 262176 | tf_op jit(solution)/shard_map/ppermute | solution.py:271
  65.6 30.7 %all_to_all.30 = bf16[4,4,1024,128]{3,2,1,0:T(8,128)(2,1)S(1)} all-to-all(bf16[4,4,1024,128]{3,2,1,0:T(8,128)(2,1)S(1)} %broadcast_in_dim.15), channel_id=1, replica_groups={{0,4,8,12},{1,5,9,13},{2,6,10,14},{3,7,11,15},{16,17,18,19},{20,21,22,2..., dimensions={0} | all-to-all | bytes 8388608 | tf_op jit(solution)/shard_map/all_to_all | solution.py:280
  96.3 5.0 %shard_map.123 = bf16[16,1024,128]{2,1,0:T(8,128)(2,1)S(1)} custom-call(s32[1]{0:T(128)} %bitcast.me_ref, bf16[16,1024,128]{2,1,0:T(8,128)(2,1)S(1)} %bitcast.28, bf16[2048,256]{1,0:T(8,128)(2,1)S(1)} %bitcast.34, bf16[2048,256]{1,0:T(8,128)(2,1)S(1)} %bitcast.35, bf16[256,2048]{1,0:T(8,128)(2,1)S(1)} %bitcast.36), custom_call_target="tpu_custom_call" | custom-call | flops 3221225472 | bytes 11534336 | tf_op jit(solution)/shard_map/pallas_call | solution.py:100
  101.3 29.2 %all_to_all.31 = bf16[4,4,1024,128]{3,2,1,0:T(8,128)(2,1)S(1)} all-to-all(bf16[4,4,1024,128]{3,2,1,0:T(8,128)(2,1)S(1)} %bitcast.29), channel_id=1, replica_groups={{0,1,2,3},{4,5,6,7},{8,9,10,11},{12,13,14,15},{16,20,24,28},{17,21,25,2..., dimensions={0} | all-to-all | bytes 8388608 | tf_op jit(solution)/shard_map/all_to_all | solution.py:280
  130.5 3.1 %shard_map.124 = bf16[4096,128]{1,0:T(8,128)(2,1)} custom-call(bf16[4,4096,128]{2,1,0:T(8,128)(2,1)S(1)} %bitcast.27), custom_call_target="tpu_custom_call" | custom-call | tf_op jit(solution)/shard_map/pallas_call | solution.py:181
  133.6 3.5 %all-to-all-start.4 = ((bf16[4,1024,128]{2,1,0:T(8,128)(2,1)}), bf16[4,1024,128]{2,1,0:T(8,128)(2,1)S(1)}, u32[]{:S(2)}, u32[]{:S(2)}) async-start(bf16[4,1024,128]{2,1,0:T(8,128)(2,1)} %bitcast.16), calls=%async_computation.4 | async-start | bytes 2097152 | tf_op jit(solution)/shard_map/all_to_all | solution.py:280
  137.1 4.5 %collective-permute-start.5 = (bf16[8,32,2048]{2,1,0:T(8,128)(2,1)S(1)}, bf16[8,32,2048]{2,1,0:T(8,128)(2,1)}, u32[]{:S(2)}, u32[]{:S(2)}) collective-permute-start(bf16[8,32,2048]{2,1,0:T(8,128)(2,1)S(1)} %pad_maximum_fusion.refs_1_), channel_id=1, source_target_pairs={{0,12},{1,13},{2,14},{3,15},{4,0},{5,1},{6,2},{7,3},{8,4},{9,5},{1... | collective-permute-start | bytes 3145736 | tf_op jit(solution)/shard_map/ppermute | solution.py:271
  143.6 3.2 %all-to-all-done.4.in_ref = bf16[4,1024,128]{2,1,0:T(8,128)(2,1)S(1)} async-done(((bf16[4,1024,128]{2,1,0:T(8,128)(2,1)}), bf16[4,1024,128]{2,1,0:T(8,128)(2,1)S(1)}, u32[]{:S(2)}, u32[]{:S(2)}) %all-to-all-start.4) | async-done | bytes 1048608 | tf_op jit(solution)/shard_map/all_to_all | solution.py:280
  147.7 5.1 %all-to-all-start.5 = ((bf16[16,2,32,128]{3,2,1,0:T(8,128)(2,1)}), bf16[16,2,32,128]{3,2,1,0:T(8,128)(2,1)}, u32[]{:S(2)}, u32[]{:S(2)}) async-start(bf16[16,2,32,128]{3,2,1,0:T(8,128)(2,1)} %bitcast.17), calls=%async_computation.5 | async-start | bytes 524288 | tf_op jit(solution)/shard_map/all_to_all | solution.py:302
  152.8 2.5 %collective-permute-start.8 = (bf16[8,32,2048]{2,1,0:T(8,128)(2,1)S(1)}, bf16[8,32,2048]{2,1,0:T(8,128)(2,1)S(1)}, u32[]{:S(2)}, u32[]{:S(2)}) collective-permute-start(bf16[8,32,2048]{2,1,0:T(8,128)(2,1)S(1)} %pad_maximum_fusion.refs_1_), channel_id=1, source_target_pairs={{0,8},{1,9},{2,10},{3,11},{4,12},{5,13},{6,14},{7,15},{8,0},{9,1},... | collective-permute-start | bytes 3145736 | tf_op jit(solution)/shard_map/ppermute | solution.py:271
  158.8 3.3 %shard_map.126.refs_2_ = f32[128,2048]{1,0:T(8,128)S(1)} custom-call(s32[1]{0:T(128)} %bitcast.me_ref, bf16[16,64,128]{2,1,0:T(8,128)(2,1)S(1)} %bitcast.30, bf16[8,32,2048]{2,1,0:T(8,128)(2,1)S(1)} %pad_maximum_fusion.refs_1_, bf16[8,32,2048]{2,1,0:T(8,128)(2,1)} %collective-permute-done.5.refs_2_, bf16[8,32,2048]{2,1,0:T(8,128)(2,1)} %collective-permute-done.6.refs_3_), custom_call_target="tpu_custom_call" | custom-call | flops 402653184 | bytes 4456448 | tf_op jit(solution)/shard_map/pallas_call | solution.py:155
  162.1 3.6 %all-to-all-done.5 = bf16[16,2,32,128]{3,2,1,0:T(8,128)(2,1)} async-done(((bf16[16,2,32,128]{3,2,1,0:T(8,128)(2,1)}), bf16[16,2,32,128]{3,2,1,0:T(8,128)(2,1)}, u32[]{:S(2)}, u32[]{:S(2)}) %all-to-all-start.5) | async-done | bytes 262176 | tf_op jit(solution)/shard_map/all_to_all | solution.py:302
  167.4 9.0 %collective-permute-start.7 = (bf16[512,128]{1,0:T(8,128)(2,1)}, bf16[512,128]{1,0:T(8,128)(2,1)}, u32[]{:S(2)}, u32[]{:S(2)}) collective-permute-start(bf16[512,128]{1,0:T(8,128)(2,1)} %bitcast.19), channel_id=1, source_target_pairs={{0,16},{16,0},{1,17},{17,1},{2,18},{18,2},{3,19},{19,3},{4,20},{20... | collective-permute-start | bytes 393224 | tf_op jit(solution)/shard_map/ppermute | solution.py:309
  177.2 2.4 %shard_map.127 = bf16[2048,128]{1,0:T(8,128)(2,1)} custom-call(s32[1]{0:T(128)} %bitcast.me_ref, bf16[16,64,128]{2,1,0:T(8,128)(2,1)S(1)} %bitcast.31, bf16[8,32,2048]{2,1,0:T(8,128)(2,1)S(1)} %collective-permute-done.8.refs_1_, f32[128,2048]{1,0:T(8,128)S(1)} %shard_map.126.refs_2_), custom_call_target="tpu_custom_call" | custom-call | flops 134217728 | bytes 2359296 | tf_op jit(solution)/shard_map/pallas_call | solution.py:155
  181.2 2.1 %shard_map.128 = bf16[256,128]{1,0:T(8,128)(2,1)} custom-call(s32[2,256]{1,0:T(2,128)S(1)} %copy-done.5, f32[256,2]{1,0:T(8,128)S(1)} %copy.21.weights_ref, bf16[512,128]{1,0:T(8,128)(2,1)S(1)} %bitcast.32, bf16[512,128]{1,0:T(8,128)(2,1)} %collective-permute-done.7.other_ref), custom_call_target="tpu_custom_call" | custom-call | tf_op jit(solution)/shard_map/pallas_call | solution.py:314
  (46 shorter events, 19.9 us)
Async XLA Ops:
  0.6 24.7 %copy-start = (f32[3,1024]{1,0:T(4,128)S(1)}, f32[3,1024]{1,0:T(4,128)}, u32[]{:S(2)}) copy-start(f32[3,1024]{1,0:T(4,128)} %param.14) | copy-start | bytes 36868
  0.7 0.8 copy-start.3
  1.5 0.7 copy-start.6
  2.2 45.8 %copy-start.10 = (bf16[64,2048]{1,0:T(8,128)(2,1)S(1)}, bf16[64,2048]{1,0:T(8,128)(2,1)}, u32[]{:S(2)}) copy-start(bf16[64,2048]{1,0:T(8,128)(2,1)} %param.12) | copy-start | bytes 786436
  3.4 0.6 copy-start.4
  4.0 29.5 %all-to-all-start = ((bf16[16,2,32,128]{3,2,1,0:T(8,128)(2,1)}), bf16[16,2,32,128]{3,2,1,0:T(8,128)(2,1)S(1)}, u32[]{:S(2)}, u32[]{:S(2)}) async-start(bf16[16,2,32,128]{3,2,1,0:T(8,128)(2,1)} %bitcast.2), calls=%async_computation | async-start | bytes 524288 | tf_op jit(solution)/shard_map/all_to_all | solution.py:235
  20.9 20.8 %collective-permute-start.1 = (bf16[64,2]{1,0:T(8,128)(2,1)S(1)}, bf16[64,2]{1,0:T(8,128)(2,1)S(1)}, u32[]{:S(2)}, u32[]{:S(2)}) collective-permute-start(bf16[64,2]{1,0:T(8,128)(2,1)S(1)} %slice.46), channel_id=1, source_target_pairs={{0,16},{16,32},{32,48},{48,64},{64,80},{80,96},{96,112},{112,128},... | collective-permute-start | bytes 776 | tf_op jit(solution)/shard_map/ppermute | solution.py:245
  33.5 9.1 %collective-permute-start = (bf16[16,32,128]{2,1,0:T(8,128)(2,1)S(1)}, bf16[16,32,128]{2,1,0:T(8,128)(2,1)S(1)}, u32[]{:S(2)}, u32[]{:S(2)}) collective-permute-start(bf16[16,32,128]{2,1,0:T(8,128)(2,1)S(1)} %get-tuple-element.31), channel_id=1, source_target_pairs={{0,16},{16,0},{1,17},{17,1},{2,18},{18,2},{3,19},{19,3},{4,20},{20... | collective-permute-start | bytes 393224 | tf_op jit(solution)/shard_map/ppermute | solution.py:284
  43.8 21.0 %all-to-all-start.1 = ((bf16[4,1024,128]{2,1,0:T(8,128)(2,1)}), bf16[4,1024,128]{2,1,0:T(8,128)(2,1)S(1)}, u32[]{:S(2)}, u32[]{:S(2)}) async-start(bf16[4,1024,128]{2,1,0:T(8,128)(2,1)} %broadcast_in_dim.14), calls=%async_computation.1 | async-start | bytes 2097152 | tf_op jit(solution)/shard_map/all_to_all | solution.py:280
  48.3 11.0 %collective-permute-start.2 = (bf16[2,32,2048]{2,1,0:T(8,128)(2,1)S(1)}, bf16[2,32,2048]{2,1,0:T(8,128)(2,1)S(1)}, u32[]{:S(2)}, u32[]{:S(2)}) collective-permute-start(bf16[2,32,2048]{2,1,0:T(8,128)(2,1)S(1)} %bitcast.38), channel_id=1, source_target_pairs={{0,3},{1,0},{2,1},{3,2},{4,7},{5,4},{6,5},{7,6},{8,11},{9,8},{10,9... | collective-permute-start | bytes 786440 | tf_op jit(solution)/shard_map/ppermute | solution.py:271
  52.9 8.9 %collective-permute-start.3 = (bf16[2,32,2048]{2,1,0:T(8,128)(2,1)S(1)}, bf16[2,32,2048]{2,1,0:T(8,128)(2,1)S(1)}, u32[]{:S(2)}, u32[]{:S(2)}) collective-permute-start(bf16[2,32,2048]{2,1,0:T(8,128)(2,1)S(1)} %bitcast.39), channel_id=1, source_target_pairs={{0,2},{1,3},{2,0},{3,1},{4,6},{5,7},{6,4},{7,5},{8,10},{9,11},{10,... | collective-permute-start | bytes 786440 | tf_op jit(solution)/shard_map/ppermute | solution.py:271
  55.4 9.2 %collective-permute-start.4 = (bf16[2,32,2048]{2,1,0:T(8,128)(2,1)S(1)}, bf16[2,32,2048]{2,1,0:T(8,128)(2,1)S(1)}, u32[]{:S(2)}, u32[]{:S(2)}) collective-permute-start(bf16[2,32,2048]{2,1,0:T(8,128)(2,1)S(1)} %bitcast.40), channel_id=1, source_target_pairs={{0,1},{1,2},{2,3},{3,0},{4,5},{5,6},{6,7},{7,4},{8,9},{9,10},{10,1... | collective-permute-start | bytes 786440 | tf_op jit(solution)/shard_map/ppermute | solution.py:271
  65.6 30.7 %copy-start.7 = (bf16[1,2048,256]{2,1,0:T(8,128)(2,1)S(1)}, bf16[1,2048,256]{2,1,0:T(8,128)(2,1)}, u32[]{:S(2)}) copy-start(bf16[1,2048,256]{2,1,0:T(8,128)(2,1)} %param.19) | copy-start | bytes 3145732
  65.6 30.7 %copy-start.8 = (bf16[1,2048,256]{2,1,0:T(8,128)(2,1)S(1)}, bf16[1,2048,256]{2,1,0:T(8,128)(2,1)}, u32[]{:S(2)}) copy-start(bf16[1,2048,256]{2,1,0:T(8,128)(2,1)} %param.20) | copy-start | bytes 3145732
  65.6 30.7 %copy-start.9 = (bf16[1,256,2048]{2,1,0:T(8,128)(2,1)S(1)}, bf16[1,256,2048]{2,1,0:T(8,128)(2,1)}, u32[]{:S(2)}) copy-start(bf16[1,256,2048]{2,1,0:T(8,128)(2,1)} %param.21) | copy-start | bytes 3145732
  130.4 28.4 %copy-start.1 = (bf16[1024,128]{1,0:T(8,128)(2,1)S(1)}, bf16[1024,128]{1,0:T(8,128)(2,1)}, u32[]{:S(2)}) copy-start(bf16[1024,128]{1,0:T(8,128)(2,1)} %param.15) | copy-start | bytes 786436
  133.6 13.2 %all-to-all-start.4 = ((bf16[4,1024,128]{2,1,0:T(8,128)(2,1)}), bf16[4,1024,128]{2,1,0:T(8,128)(2,1)S(1)}, u32[]{:S(2)}, u32[]{:S(2)}) async-start(bf16[4,1024,128]{2,1,0:T(8,128)(2,1)} %bitcast.16), calls=%async_computation.4 | async-start | bytes 2097152 | tf_op jit(solution)/shard_map/all_to_all | solution.py:280
  137.1 19.9 %collective-permute-start.5 = (bf16[8,32,2048]{2,1,0:T(8,128)(2,1)S(1)}, bf16[8,32,2048]{2,1,0:T(8,128)(2,1)}, u32[]{:S(2)}, u32[]{:S(2)}) collective-permute-start(bf16[8,32,2048]{2,1,0:T(8,128)(2,1)S(1)} %pad_maximum_fusion.refs_1_), channel_id=1, source_target_pairs={{0,12},{1,13},{2,14},{3,15},{4,0},{5,1},{6,2},{7,3},{8,4},{9,5},{1... | collective-permute-start | bytes 3145736 | tf_op jit(solution)/shard_map/ppermute | solution.py:271
  141.7 17.2 %collective-permute-start.6 = (bf16[8,32,2048]{2,1,0:T(8,128)(2,1)S(1)}, bf16[8,32,2048]{2,1,0:T(8,128)(2,1)}, u32[]{:S(2)}, u32[]{:S(2)}) collective-permute-start(bf16[8,32,2048]{2,1,0:T(8,128)(2,1)S(1)} %pad_maximum_fusion.refs_1_), channel_id=1, source_target_pairs={{0,4},{1,5},{2,6},{3,7},{4,8},{5,9},{6,10},{7,11},{8,12},{9,13},{1... | collective-permute-start | bytes 3145736 | tf_op jit(solution)/shard_map/ppermute | solution.py:271
  147.7 17.9 %all-to-all-start.5 = ((bf16[16,2,32,128]{3,2,1,0:T(8,128)(2,1)}), bf16[16,2,32,128]{3,2,1,0:T(8,128)(2,1)}, u32[]{:S(2)}, u32[]{:S(2)}) async-start(bf16[16,2,32,128]{3,2,1,0:T(8,128)(2,1)} %bitcast.17), calls=%async_computation.5 | async-start | bytes 524288 | tf_op jit(solution)/shard_map/all_to_all | solution.py:302
  152.8 24.4 %collective-permute-start.8 = (bf16[8,32,2048]{2,1,0:T(8,128)(2,1)S(1)}, bf16[8,32,2048]{2,1,0:T(8,128)(2,1)S(1)}, u32[]{:S(2)}, u32[]{:S(2)}) collective-permute-start(bf16[8,32,2048]{2,1,0:T(8,128)(2,1)S(1)} %pad_maximum_fusion.refs_1_), channel_id=1, source_target_pairs={{0,8},{1,9},{2,10},{3,11},{4,12},{5,13},{6,14},{7,15},{8,0},{9,1},... | collective-permute-start | bytes 3145736 | tf_op jit(solution)/shard_map/ppermute | solution.py:271
  167.4 12.3 %collective-permute-start.7 = (bf16[512,128]{1,0:T(8,128)(2,1)}, bf16[512,128]{1,0:T(8,128)(2,1)}, u32[]{:S(2)}, u32[]{:S(2)}) collective-permute-start(bf16[512,128]{1,0:T(8,128)(2,1)} %bitcast.19), channel_id=1, source_target_pairs={{0,16},{16,0},{1,17},{17,1},{2,18},{18,2},{3,19},{19,3},{4,20},{20... | collective-permute-start | bytes 393224 | tf_op jit(solution)/shard_map/ppermute | solution.py:309
  179.6 0.9 copy-start.2
  180.5 0.7 copy-start.5
where the time goes:
time: 184 us; the launch traced here: 183 us
  starting transfers between devices  68.5 us (37%)
  blocking collectives  59.9 us (33%)
  waiting for transfers between devices  26 us (14%)
  Pallas kernels  18 us (10%)
  local copies, waits for them, and re-layouts  8.32 us (5%)
    all_to_all x2, blocking collectives, exchange(): lax.all_to_all(value, ('c', 'tp'), 0, 0, axis_index_groups=groups, tiled=...  59.9 us
    ppermute x6, starting transfers between devices, step(): return lax.ppermute(value, ('c', 'tp'), pairs)  18.5 us
    all_to_all x1, starting transfers between devices, layer(): lax.all_to_all(outgoing.reshape(depth, 2, capacity, cols_part), 'z', 0, 0...  15.7 us
    ppermute x6, waiting for transfers between devices, step(): return lax.ppermute(value, ('c', 'tp'), pairs)  10.3 us
    ppermute x1, starting transfers between devices, layer(): lax.ppermute(returned[:, 1].reshape(half, cols_part), 'c', swap)  8.99 us
    ppermute x1, starting transfers between devices, layer(): rows_other = lax.ppermute(arrived[:, 1], 'c', swap)  8.12 us
    all_to_all x1, waiting for transfers between devices, layer(): lax.all_to_all(outgoing.reshape(depth, 2, capacity, cols_part), 'z', 0, 0...  8.12 us
    all_to_all x2, starting transfers between devices, exchange(): lax.all_to_all(value, ('c', 'tp'), 0, 0, axis_index_groups=groups, tiled=...  7.7 us
  transfers between devices with their start and end apart: 13, of which 9 were waited for; matrix products, arithmetic and copies ran while one was open for 2% of the time, Pallas kernels for 4%

commit v1 on v0

--- a/solution.py
+++ b/solution.py
@@ -291,14 +291,15 @@
     part = expert_part(me, x, *weights, rows_b)
     part = part.reshape(side, side, slot_total, cols_part)
     half_sums = exchange(part, early).reshape(side, side * slot_total, cols_part)
-    half_sums = sum_parts(half_sums, 8).reshape(side, slot_total, cols_part)
+    half_sums = sum_parts(half_sums, 4).reshape(side, slot_total, cols_part)
     half_sums, line = lax.optimization_barrier((half_sums, line))
     line_before = step(line, 1, 1)
     line_after = step(line, -1, 1)
-    line_far = step(line, 2, 1)
     expert_rows = exchange(half_sums, late)
     expert_rows = sum_parts(expert_rows, 2)
     back = expert_rows.reshape(depth, 2, capacity, cols_part)
+    line_far_a = step(line_before[:4], 1, 1)
+    line_far_b = step(line_after[4:], -1, 1)
     returned = lax.all_to_all(back, "z", 0, 0, tiled=True)
     blocks = mixer_proj.reshape(tp, width_part, cols_part)
     most = mixer_product(
@@ -308,7 +309,7 @@
     returned_own = returned[:, 0].reshape(half, cols_part)
     returned_other = lax.ppermute(returned[:, 1].reshape(half, cols_part), "c", swap)
     mixed_out = mixer_product(
-        me, blocks, (line_far,), (2,), most, length // 4
+        me, blocks, (line_far_a, line_far_b), (2,), most, length // 2
     )
     returned_other, mixed_out = lax.optimization_barrier((returned_other, mixed_out))
     expert_out = pl.pallas_call(

time: 184 us -> 183 us (level)
  starting transfers between devices: 68.5 us -> 71.7 us
  Pallas kernels: 18 us -> 15.3 us
  waiting for transfers between devices: 26 us -> 24 us
    ppermute x6 -> x7, starting transfers between devices: 18.5 us -> 22.6 us  [step(): return lax.ppermute(value, ('c', 'tp'), pairs)]
    all_to_all x1, waiting for transfers between devices: 3.58 us -> 0.01 us  [layer(): returned = lax.all_to_all(back, 'z', 0, 0, tiled=True)]
    slice x0 -> x2, local copies, waits for them, and re-layouts: none -> 2.73 us  [the longest x1 1.9 us: layer(): line_far_b = step(line_after[4:], -1, 1)]
    unnamed x23 -> x21, local copies, waits for them, and re-layouts: 4.52 us -> 2.39 us
    ppermute x6 -> x7, waiting for transfers between devices: 10.3 us -> 11.8 us  [step(): return lax.ppermute(value, ('c', 'tp'), pairs)]
  transfers between devices with their start and end apart: 13 -> 14, of which waited for: 9 -> 7; matrix products, arithmetic and copies ran while one was open for 2% -> 3% of each run, Pallas kernels for 4% -> 3%
where the time goes in v1:
time: 183 us; the launch traced here: 182 us
  starting transfers between devices  71.7 us (39%)
  blocking collectives  59.9 us (33%)
  waiting for transfers between devices  24 us (13%)
  Pallas kernels  15.3 us (8%)
  local copies, waits for them, and re-layouts  8.22 us (4%)
    all_to_all x2, blocking collectives, exchange(): lax.all_to_all(value, ('c', 'tp'), 0, 0, axis_index_groups=groups, tiled=...  59.9 us
    ppermute x7, starting transfers between devices, step(): return lax.ppermute(value, ('c', 'tp'), pairs)  22.6 us
    all_to_all x1, starting transfers between devices, layer(): lax.all_to_all(outgoing.reshape(depth, 2, capacity, cols_part), 'z', 0, 0...  15.7 us
    ppermute x7, waiting for transfers between devices, step(): return lax.ppermute(value, ('c', 'tp'), pairs)  11.8 us
    ppermute x1, starting transfers between devices, layer(): rows_other = lax.ppermute(arrived[:, 1], 'c', swap)  8.12 us
    all_to_all x1, waiting for transfers between devices, layer(): lax.all_to_all(outgoing.reshape(depth, 2, capacity, cols_part), 'z', 0, 0...  8.12 us
    ppermute x1, starting transfers between devices, layer(): lax.ppermute(returned[:, 1].reshape(half, cols_part), 'c', swap)  7.93 us
    all_to_all x2, starting transfers between devices, exchange(): lax.all_to_all(value, ('c', 'tp'), 0, 0, axis_index_groups=groups, tiled=...  7.83 us
  transfers between devices with their start and end apart: 14, of which 7 were waited for; matrix products, arithmetic and copies ran while one was open for 3% of the time, Pallas kernels for 3%

profile of v1, /device:TPU:1, one launch (start us, length us, event | category | flops | bytes accessed | tf_op | source)
XLA Modules:
  0.0 181.7 jit_solution(15407888449089467120)
XLA Ops:
  3.4 15.7 %all-to-all-start = ((bf16[16,2,32,128]{3,2,1,0:T(8,128)(2,1)}), bf16[16,2,32,128]{3,2,1,0:T(8,128)(2,1)S(1)}, u32[]{:S(2)}, u32[]{:S(2)}) async-start(bf16[16,2,32,128]{3,2,1,0:T(8,128)(2,1)} %bitcast.2), calls=%async_computation | async-start | bytes 524288 | tf_op jit(solution)/shard_map/all_to_all | solution.py:235
  20.3 4.4 %collective-permute-start.1 = (bf16[64,2]{1,0:T(8,128)(2,1)S(1)}, bf16[64,2]{1,0:T(8,128)(2,1)S(1)}, u32[]{:S(2)}, u32[]{:S(2)}) collective-permute-start(bf16[64,2]{1,0:T(8,128)(2,1)S(1)} %slice.54), channel_id=1, source_target_pairs={{0,16},{16,32},{32,48},{48,64},{64,80},{80,96},{96,112},{112,128},... | collective-permute-start | bytes 776 | tf_op jit(solution)/shard_map/ppermute | solution.py:245
  24.8 8.1 %all-to-all-done = bf16[16,2,32,128]{3,2,1,0:T(8,128)(2,1)S(1)} async-done(((bf16[16,2,32,128]{3,2,1,0:T(8,128)(2,1)}), bf16[16,2,32,128]{3,2,1,0:T(8,128)(2,1)S(1)}, u32[]{:S(2)}, u32[]{:S(2)}) %all-to-all-start) | async-done | bytes 262176 | tf_op jit(solution)/shard_map/all_to_all | solution.py:235
  32.9 8.1 %collective-permute-start = (bf16[16,32,128]{2,1,0:T(8,128)(2,1)S(1)}, bf16[16,32,128]{2,1,0:T(8,128)(2,1)S(1)}, u32[]{:S(2)}, u32[]{:S(2)}) collective-permute-start(bf16[16,32,128]{2,1,0:T(8,128)(2,1)S(1)} %get-tuple-element.31), channel_id=1, source_target_pairs={{0,16},{16,0},{1,17},{17,1},{2,18},{18,2},{3,19},{19,3},{4,20},{20... | collective-permute-start | bytes 393224 | tf_op jit(solution)/shard_map/ppermute | solution.py:284
  43.2 4.2 %all-to-all-start.1 = ((bf16[4,1024,128]{2,1,0:T(8,128)(2,1)}), bf16[4,1024,128]{2,1,0:T(8,128)(2,1)S(1)}, u32[]{:S(2)}, u32[]{:S(2)}) async-start(bf16[4,1024,128]{2,1,0:T(8,128)(2,1)} %broadcast_in_dim.14), calls=%async_computation.1 | async-start | bytes 2097152 | tf_op jit(solution)/shard_map/all_to_all | solution.py:280
  47.7 4.6 %collective-permute-start.2 = (bf16[2,32,2048]{2,1,0:T(8,128)(2,1)S(1)}, bf16[2,32,2048]{2,1,0:T(8,128)(2,1)S(1)}, u32[]{:S(2)}, u32[]{:S(2)}) collective-permute-start(bf16[2,32,2048]{2,1,0:T(8,128)(2,1)S(1)} %bitcast.39), channel_id=1, source_target_pairs={{0,3},{1,0},{2,1},{3,2},{4,7},{5,4},{6,5},{7,6},{8,11},{9,8},{10,9... | collective-permute-start | bytes 786440 | tf_op jit(solution)/shard_map/ppermute | solution.py:271
  52.3 2.5 %collective-permute-start.3 = (bf16[2,32,2048]{2,1,0:T(8,128)(2,1)S(1)}, bf16[2,32,2048]{2,1,0:T(8,128)(2,1)S(1)}, u32[]{:S(2)}, u32[]{:S(2)}) collective-permute-start(bf16[2,32,2048]{2,1,0:T(8,128)(2,1)S(1)} %bitcast.40), channel_id=1, source_target_pairs={{0,2},{1,3},{2,0},{3,1},{4,6},{5,7},{6,4},{7,5},{8,10},{9,11},{10,... | collective-permute-start | bytes 786440 | tf_op jit(solution)/shard_map/ppermute | solution.py:271
  54.8 2.5 %collective-permute-start.4 = (bf16[2,32,2048]{2,1,0:T(8,128)(2,1)S(1)}, bf16[2,32,2048]{2,1,0:T(8,128)(2,1)S(1)}, u32[]{:S(2)}, u32[]{:S(2)}) collective-permute-start(bf16[2,32,2048]{2,1,0:T(8,128)(2,1)S(1)} %bitcast.41), channel_id=1, source_target_pairs={{0,1},{1,2},{2,3},{3,0},{4,5},{5,6},{6,7},{7,4},{8,9},{9,10},{10,1... | collective-permute-start | bytes 786440 | tf_op jit(solution)/shard_map/ppermute | solution.py:271
  58.7 2.5 %collective-permute-done.3 = bf16[2,32,2048]{2,1,0:T(8,128)(2,1)S(1)} collective-permute-done((bf16[2,32,2048]{2,1,0:T(8,128)(2,1)S(1)}, bf16[2,32,2048]{2,1,0:T(8,128)(2,1)S(1)}, u32[]{:S(2)}, u32[]{:S(2)}) %collective-permute-start.3) | collective-permute-done | bytes 262176 | tf_op jit(solution)/shard_map/ppermute | solution.py:271
  61.2 2.8 %collective-permute-done.4 = bf16[2,32,2048]{2,1,0:T(8,128)(2,1)S(1)} collective-permute-done((bf16[2,32,2048]{2,1,0:T(8,128)(2,1)S(1)}, bf16[2,32,2048]{2,1,0:T(8,128)(2,1)S(1)}, u32[]{:S(2)}, u32[]{:S(2)}) %collective-permute-start.4) | collective-permute-done | bytes 262176 | tf_op jit(solution)/shard_map/ppermute | solution.py:271
  65.0 30.7 %all_to_all.30 = bf16[4,4,1024,128]{3,2,1,0:T(8,128)(2,1)S(1)} all-to-all(bf16[4,4,1024,128]{3,2,1,0:T(8,128)(2,1)S(1)} %broadcast_in_dim.15), channel_id=1, replica_groups={{0,4,8,12},{1,5,9,13},{2,6,10,14},{3,7,11,15},{16,17,18,19},{20,21,22,2..., dimensions={0} | all-to-all | bytes 8388608 | tf_op jit(solution)/shard_map/all_to_all | solution.py:280
  95.7 5.0 %shard_map.123 = bf16[16,1024,128]{2,1,0:T(8,128)(2,1)S(1)} custom-call(s32[1]{0:T(128)} %bitcast.me_ref, bf16[16,1024,128]{2,1,0:T(8,128)(2,1)S(1)} %bitcast.28, bf16[2048,256]{1,0:T(8,128)(2,1)S(1)} %bitcast.35, bf16[2048,256]{1,0:T(8,128)(2,1)S(1)} %bitcast.36, bf16[256,2048]{1,0:T(8,128)(2,1)S(1)} %bitcast.37), custom_call_target="tpu_custom_call" | custom-call | flops 3221225472 | bytes 11534336 | tf_op jit(solution)/shard_map/pallas_call | solution.py:100
  100.7 29.2 %all_to_all.31 = bf16[4,4,1024,128]{3,2,1,0:T(8,128)(2,1)S(1)} all-to-all(bf16[4,4,1024,128]{3,2,1,0:T(8,128)(2,1)S(1)} %bitcast.29), channel_id=1, replica_groups={{0,1,2,3},{4,5,6,7},{8,9,10,11},{12,13,14,15},{16,20,24,28},{17,21,25,2..., dimensions={0} | all-to-all | bytes 8388608 | tf_op jit(solution)/shard_map/all_to_all | solution.py:280
  129.9 2.0 %shard_map.124 = bf16[4096,128]{1,0:T(8,128)(2,1)} custom-call(bf16[4,4096,128]{2,1,0:T(8,128)(2,1)S(1)} %bitcast.27), custom_call_target="tpu_custom_call" | custom-call | tf_op jit(solution)/shard_map/pallas_call | solution.py:181
  131.9 3.6 %all-to-all-start.4 = ((bf16[4,1024,128]{2,1,0:T(8,128)(2,1)}), bf16[4,1024,128]{2,1,0:T(8,128)(2,1)S(1)}, u32[]{:S(2)}, u32[]{:S(2)}) async-start(bf16[4,1024,128]{2,1,0:T(8,128)(2,1)} %bitcast.16), calls=%async_computation.4 | async-start | bytes 2097152 | tf_op jit(solution)/shard_map/all_to_all | solution.py:280
  135.6 3.4 %collective-permute-start.6 = (bf16[8,32,2048]{2,1,0:T(8,128)(2,1)S(1)}, bf16[8,32,2048]{2,1,0:T(8,128)(2,1)S(1)}, u32[]{:S(2)}, u32[]{:S(2)}) collective-permute-start(bf16[8,32,2048]{2,1,0:T(8,128)(2,1)S(1)} %pad_maximum_fusion.refs_1_), channel_id=1, source_target_pairs={{0,4},{1,5},{2,6},{3,7},{4,8},{5,9},{6,10},{7,11},{8,12},{9,13},{1... | collective-permute-start | bytes 3145736 | tf_op jit(solution)/shard_map/ppermute | solution.py:271
  139.0 3.1 %collective-permute-start.5 = (bf16[8,32,2048]{2,1,0:T(8,128)(2,1)S(1)}, bf16[8,32,2048]{2,1,0:T(8,128)(2,1)}, u32[]{:S(2)}, u32[]{:S(2)}) collective-permute-start(bf16[8,32,2048]{2,1,0:T(8,128)(2,1)S(1)} %pad_maximum_fusion.refs_1_), channel_id=1, source_target_pairs={{0,12},{1,13},{2,14},{3,15},{4,0},{5,1},{6,2},{7,3},{8,4},{9,5},{1... | collective-permute-start | bytes 3145736 | tf_op jit(solution)/shard_map/ppermute | solution.py:271
  142.2 3.2 %all-to-all-done.4.in_ref = bf16[4,1024,128]{2,1,0:T(8,128)(2,1)S(1)} async-done(((bf16[4,1024,128]{2,1,0:T(8,128)(2,1)}), bf16[4,1024,128]{2,1,0:T(8,128)(2,1)S(1)}, u32[]{:S(2)}, u32[]{:S(2)}) %all-to-all-start.4) | async-done | bytes 1048608 | tf_op jit(solution)/shard_map/all_to_all | solution.py:280
  146.4 5.1 %all-to-all-start.5 = ((bf16[16,2,32,128]{3,2,1,0:T(8,128)(2,1)}), bf16[16,2,32,128]{3,2,1,0:T(8,128)(2,1)}, u32[]{:S(2)}, u32[]{:S(2)}) async-start(bf16[16,2,32,128]{3,2,1,0:T(8,128)(2,1)} %bitcast.32), calls=%async_computation.5 | async-start | bytes 524288 | tf_op jit(solution)/shard_map/all_to_all | solution.py:303
  151.4 5.1 %collective-permute-done.6.refs_3_ = bf16[8,32,2048]{2,1,0:T(8,128)(2,1)S(1)} collective-permute-done((bf16[8,32,2048]{2,1,0:T(8,128)(2,1)S(1)}, bf16[8,32,2048]{2,1,0:T(8,128)(2,1)S(1)}, u32[]{:S(2)}, u32[]{:S(2)}) %collective-permute-start.6) | collective-permute-done | bytes 1048608 | tf_op jit(solution)/shard_map/ppermute | solution.py:271
  161.2 4.6 %collective-permute-start.9 = (bf16[4,32,2048]{2,1,0:T(8,128)(2,1)}, bf16[4,32,2048]{2,1,0:T(8,128)(2,1)}, u32[]{:S(2)}, u32[]{:S(2)}) collective-permute-start(bf16[4,32,2048]{2,1,0:T(8,128)(2,1)} %slice.59), channel_id=1, source_target_pairs={{0,12},{1,13},{2,14},{3,15},{4,0},{5,1},{6,2},{7,3},{8,4},{9,5},{1... | collective-permute-start | bytes 1572872 | tf_op jit(solution)/shard_map/ppermute | solution.py:271
  165.8 3.1 %shard_map.126.refs_3_ = f32[128,2048]{1,0:T(8,128)S(1)} custom-call(s32[1]{0:T(128)} %bitcast.me_ref, bf16[16,64,128]{2,1,0:T(8,128)(2,1)S(1)} %bitcast.30, bf16[8,32,2048]{2,1,0:T(8,128)(2,1)S(1)} %pad_maximum_fusion.refs_1_, bf16[8,32,2048]{2,1,0:T(8,128)(2,1)} %collective-permute-done.5.refs_2_, bf16[8,32,2048]{2,1,0:T(8,128)(2,1)S(1)} %collective-permute-done.6.refs_3_), custom_call_target="tpu_custom_call" | custom-call | flops 402653184 | bytes 4456448 | tf_op jit(solution)/shard_map/pallas_call | solution.py:155
  169.9 7.9 %collective-permute-start.7 = (bf16[512,128]{1,0:T(8,128)(2,1)S(1)}, bf16[512,128]{1,0:T(8,128)(2,1)S(1)}, u32[]{:S(2)}, u32[]{:S(2)}) collective-permute-start(bf16[512,128]{1,0:T(8,128)(2,1)S(1)} %bitcast.43), channel_id=1, source_target_pairs={{0,16},{16,0},{1,17},{17,1},{2,18},{18,2},{3,19},{19,3},{4,20},{20... | collective-permute-start | bytes 393224 | tf_op jit(solution)/shard_map/ppermute | solution.py:310
  178.0 2.5 %shard_map.127 = bf16[2048,128]{1,0:T(8,128)(2,1)} custom-call(s32[1]{0:T(128)} %bitcast.me_ref, bf16[16,64,128]{2,1,0:T(8,128)(2,1)S(1)} %bitcast.31, bf16[4,32,2048]{2,1,0:T(8,128)(2,1)} %collective-permute-done.8.refs_1_, bf16[4,32,2048]{2,1,0:T(8,128)(2,1)} %collective-permute-done.9.refs_2_, f32[128,2048]{1,0:T(8,128)S(1)} %shard_map.126.refs_3_), custom_call_target="tpu_custom_call" | custom-call | flops 134217728 | bytes 2359296 | tf_op jit(solution)/shard_map/pallas_call | solution.py:155
  (48 shorter events, 16.8 us)
Async XLA Ops:
  0.6 24.1 %copy-start = (f32[3,1024]{1,0:T(4,128)S(1)}, f32[3,1024]{1,0:T(4,128)}, u32[]{:S(2)}) copy-start(f32[3,1024]{1,0:T(4,128)} %param.14) | copy-start | bytes 36868
  0.7 0.8 copy-start.3
  1.5 0.7 copy-start.4
  2.2 45.2 %copy-start.8 = (bf16[64,2048]{1,0:T(8,128)(2,1)S(1)}, bf16[64,2048]{1,0:T(8,128)(2,1)}, u32[]{:S(2)}) copy-start(bf16[64,2048]{1,0:T(8,128)(2,1)} %param.12) | copy-start | bytes 786436
  3.4 29.5 %all-to-all-start = ((bf16[16,2,32,128]{3,2,1,0:T(8,128)(2,1)}), bf16[16,2,32,128]{3,2,1,0:T(8,128)(2,1)S(1)}, u32[]{:S(2)}, u32[]{:S(2)}) async-start(bf16[16,2,32,128]{3,2,1,0:T(8,128)(2,1)} %bitcast.2), calls=%async_computation | async-start | bytes 524288 | tf_op jit(solution)/shard_map/all_to_all | solution.py:235
  20.3 20.8 %collective-permute-start.1 = (bf16[64,2]{1,0:T(8,128)(2,1)S(1)}, bf16[64,2]{1,0:T(8,128)(2,1)S(1)}, u32[]{:S(2)}, u32[]{:S(2)}) collective-permute-start(bf16[64,2]{1,0:T(8,128)(2,1)S(1)} %slice.54), channel_id=1, source_target_pairs={{0,16},{16,32},{32,48},{48,64},{64,80},{80,96},{96,112},{112,128},... | collective-permute-start | bytes 776 | tf_op jit(solution)/shard_map/ppermute | solution.py:245
  32.9 9.1 %collective-permute-start = (bf16[16,32,128]{2,1,0:T(8,128)(2,1)S(1)}, bf16[16,32,128]{2,1,0:T(8,128)(2,1)S(1)}, u32[]{:S(2)}, u32[]{:S(2)}) collective-permute-start(bf16[16,32,128]{2,1,0:T(8,128)(2,1)S(1)} %get-tuple-element.31), channel_id=1, source_target_pairs={{0,16},{16,0},{1,17},{17,1},{2,18},{18,2},{3,19},{19,3},{4,20},{20... | collective-permute-start | bytes 393224 | tf_op jit(solution)/shard_map/ppermute | solution.py:284
  43.2 21.0 %all-to-all-start.1 = ((bf16[4,1024,128]{2,1,0:T(8,128)(2,1)}), bf16[4,1024,128]{2,1,0:T(8,128)(2,1)S(1)}, u32[]{:S(2)}, u32[]{:S(2)}) async-start(bf16[4,1024,128]{2,1,0:T(8,128)(2,1)} %broadcast_in_dim.14), calls=%async_computation.1 | async-start | bytes 2097152 | tf_op jit(solution)/shard_map/all_to_all | solution.py:280
  47.7 11.0 %collective-permute-start.2 = (bf16[2,32,2048]{2,1,0:T(8,128)(2,1)S(1)}, bf16[2,32,2048]{2,1,0:T(8,128)(2,1)S(1)}, u32[]{:S(2)}, u32[]{:S(2)}) collective-permute-start(bf16[2,32,2048]{2,1,0:T(8,128)(2,1)S(1)} %bitcast.39), channel_id=1, source_target_pairs={{0,3},{1,0},{2,1},{3,2},{4,7},{5,4},{6,5},{7,6},{8,11},{9,8},{10,9... | collective-permute-start | bytes 786440 | tf_op jit(solution)/shard_map/ppermute | solution.py:271
  52.3 8.9 %collective-permute-start.3 = (bf16[2,32,2048]{2,1,0:T(8,128)(2,1)S(1)}, bf16[2,32,2048]{2,1,0:T(8,128)(2,1)S(1)}, u32[]{:S(2)}, u32[]{:S(2)}) collective-permute-start(bf16[2,32,2048]{2,1,0:T(8,128)(2,1)S(1)} %bitcast.40), channel_id=1, source_target_pairs={{0,2},{1,3},{2,0},{3,1},{4,6},{5,7},{6,4},{7,5},{8,10},{9,11},{10,... | collective-permute-start | bytes 786440 | tf_op jit(solution)/shard_map/ppermute | solution.py:271
  54.8 9.2 %collective-permute-start.4 = (bf16[2,32,2048]{2,1,0:T(8,128)(2,1)S(1)}, bf16[2,32,2048]{2,1,0:T(8,128)(2,1)S(1)}, u32[]{:S(2)}, u32[]{:S(2)}) collective-permute-start(bf16[2,32,2048]{2,1,0:T(8,128)(2,1)S(1)} %bitcast.41), channel_id=1, source_target_pairs={{0,1},{1,2},{2,3},{3,0},{4,5},{5,6},{6,7},{7,4},{8,9},{9,10},{10,1... | collective-permute-start | bytes 786440 | tf_op jit(solution)/shard_map/ppermute | solution.py:271
  65.0 30.7 %copy-start.5 = (bf16[1,2048,256]{2,1,0:T(8,128)(2,1)S(1)}, bf16[1,2048,256]{2,1,0:T(8,128)(2,1)}, u32[]{:S(2)}) copy-start(bf16[1,2048,256]{2,1,0:T(8,128)(2,1)} %param.19) | copy-start | bytes 3145732
  65.0 30.7 %copy-start.6 = (bf16[1,2048,256]{2,1,0:T(8,128)(2,1)S(1)}, bf16[1,2048,256]{2,1,0:T(8,128)(2,1)}, u32[]{:S(2)}) copy-start(bf16[1,2048,256]{2,1,0:T(8,128)(2,1)} %param.20) | copy-start | bytes 3145732
  65.0 30.7 %copy-start.7 = (bf16[1,256,2048]{2,1,0:T(8,128)(2,1)S(1)}, bf16[1,256,2048]{2,1,0:T(8,128)(2,1)}, u32[]{:S(2)}) copy-start(bf16[1,256,2048]{2,1,0:T(8,128)(2,1)} %param.21) | copy-start | bytes 3145732
  131.9 33.8 %copy-start.1 = (bf16[1024,128]{1,0:T(8,128)(2,1)S(1)}, bf16[1024,128]{1,0:T(8,128)(2,1)}, u32[]{:S(2)}) copy-start(bf16[1024,128]{1,0:T(8,128)(2,1)} %param.15) | copy-start | bytes 786436
  131.9 13.5 %all-to-all-start.4 = ((bf16[4,1024,128]{2,1,0:T(8,128)(2,1)}), bf16[4,1024,128]{2,1,0:T(8,128)(2,1)S(1)}, u32[]{:S(2)}, u32[]{:S(2)}) async-start(bf16[4,1024,128]{2,1,0:T(8,128)(2,1)} %bitcast.16), calls=%async_computation.4 | async-start | bytes 2097152 | tf_op jit(solution)/shard_map/all_to_all | solution.py:280
  135.6 42.3 %copy-start.9 = (f32[256,2]{0,1:T(2,128)S(1)}, f32[256,2]{0,1:T(2,128)}, u32[]{:S(2)}) copy-start(f32[256,2]{0,1:T(2,128)} %param.18) | copy-start | bytes 6148
  135.6 20.9 %collective-permute-start.6 = (bf16[8,32,2048]{2,1,0:T(8,128)(2,1)S(1)}, bf16[8,32,2048]{2,1,0:T(8,128)(2,1)S(1)}, u32[]{:S(2)}, u32[]{:S(2)}) collective-permute-start(bf16[8,32,2048]{2,1,0:T(8,128)(2,1)S(1)} %pad_maximum_fusion.refs_1_), channel_id=1, source_target_pairs={{0,4},{1,5},{2,6},{3,7},{4,8},{5,9},{6,10},{7,11},{8,12},{9,13},{1... | collective-permute-start | bytes 3145736 | tf_op jit(solution)/shard_map/ppermute | solution.py:271
  139.0 20.2 %collective-permute-start.5 = (bf16[8,32,2048]{2,1,0:T(8,128)(2,1)S(1)}, bf16[8,32,2048]{2,1,0:T(8,128)(2,1)}, u32[]{:S(2)}, u32[]{:S(2)}) collective-permute-start(bf16[8,32,2048]{2,1,0:T(8,128)(2,1)S(1)} %pad_maximum_fusion.refs_1_), channel_id=1, source_target_pairs={{0,12},{1,13},{2,14},{3,15},{4,0},{5,1},{6,2},{7,3},{8,4},{9,5},{1... | collective-permute-start | bytes 3145736 | tf_op jit(solution)/shard_map/ppermute | solution.py:271
  145.6 0.7 copy-start.2
  146.4 22.5 %all-to-all-start.5 = ((bf16[16,2,32,128]{3,2,1,0:T(8,128)(2,1)}), bf16[16,2,32,128]{3,2,1,0:T(8,128)(2,1)}, u32[]{:S(2)}, u32[]{:S(2)}) async-start(bf16[16,2,32,128]{3,2,1,0:T(8,128)(2,1)} %bitcast.32), calls=%async_computation.5 | async-start | bytes 524288 | tf_op jit(solution)/shard_map/all_to_all | solution.py:303
  157.3 20.6 %collective-permute-start.8 = (bf16[4,32,2048]{2,1,0:T(8,128)(2,1)}, bf16[4,32,2048]{2,1,0:T(8,128)(2,1)}, u32[]{:S(2)}, u32[]{:S(2)}) collective-permute-start(bf16[4,32,2048]{2,1,0:T(8,128)(2,1)} %slice.58), channel_id=1, source_target_pairs={{0,4},{1,5},{2,6},{3,7},{4,8},{5,9},{6,10},{7,11},{8,12},{9,13},{1... | collective-permute-start | bytes 1572872 | tf_op jit(solution)/shard_map/ppermute | solution.py:271
  161.2 16.8 %collective-permute-start.9 = (bf16[4,32,2048]{2,1,0:T(8,128)(2,1)}, bf16[4,32,2048]{2,1,0:T(8,128)(2,1)}, u32[]{:S(2)}, u32[]{:S(2)}) collective-permute-start(bf16[4,32,2048]{2,1,0:T(8,128)(2,1)} %slice.59), channel_id=1, source_target_pairs={{0,12},{1,13},{2,14},{3,15},{4,0},{5,1},{6,2},{7,3},{8,4},{9,5},{1... | collective-permute-start | bytes 1572872 | tf_op jit(solution)/shard_map/ppermute | solution.py:271
  169.9 10.6 %collective-permute-start.7 = (bf16[512,128]{1,0:T(8,128)(2,1)S(1)}, bf16[512,128]{1,0:T(8,128)(2,1)S(1)}, u32[]{:S(2)}, u32[]{:S(2)}) collective-permute-start(bf16[512,128]{1,0:T(8,128)(2,1)S(1)} %bitcast.43), channel_id=1, source_target_pairs={{0,16},{16,0},{1,17},{17,1},{2,18},{18,2},{3,19},{19,3},{4,20},{20... | collective-permute-start | bytes 393224 | tf_op jit(solution)/shard_map/ppermute | solution.py:310

commit v2 on v1

--- a/solution.py
+++ b/solution.py
@@ -291,7 +291,7 @@
     part = expert_part(me, x, *weights, rows_b)
     part = part.reshape(side, side, slot_total, cols_part)
     half_sums = exchange(part, early).reshape(side, side * slot_total, cols_part)
-    half_sums = sum_parts(half_sums, 4).reshape(side, slot_total, cols_part)
+    half_sums = sum_parts(half_sums, 2).reshape(side, slot_total, cols_part)
     half_sums, line = lax.optimization_barrier((half_sums, line))
     line_before = step(line, 1, 1)
     line_after = step(line, -1, 1)
@@ -303,13 +303,13 @@
     returned = lax.all_to_all(back, "z", 0, 0, tiled=True)
     blocks = mixer_proj.reshape(tp, width_part, cols_part)
     most = mixer_product(
-        me, blocks, (line, line_after, line_before), (0, 1, 3), None, length // 4
+        me, blocks, (line, line_after, line_before), (0, 1, 3), None, length // 2
     )
     returned, most = lax.optimization_barrier((returned, most))
     returned_own = returned[:, 0].reshape(half, cols_part)
     returned_other = lax.ppermute(returned[:, 1].reshape(half, cols_part), "c", swap)
     mixed_out = mixer_product(
-        me, blocks, (line_far_a, line_far_b), (2,), most, length // 2
+        me, blocks, (line_far_a, line_far_b), (2,), most, length
     )
     returned_other, mixed_out = lax.optimization_barrier((returned_other, mixed_out))
     expert_out = pl.pallas_call(

time: 183 us -> 182 us (level)
  no operation moved by 1% of the time
where the time goes in v2:
time: 182 us; the launch traced here: 180 us
  starting transfers between devices  71.7 us (39%)
  blocking collectives  59.9 us (33%)
  waiting for transfers between devices  24 us (13%)
  Pallas kernels  13.7 us (8%)
  local copies, waits for them, and re-layouts  8.22 us (5%)
    all_to_all x2, blocking collectives, exchange(): lax.all_to_all(value, ('c', 'tp'), 0, 0, axis_index_groups=groups, tiled=...  59.9 us
    ppermute x7, starting transfers between devices, step(): return lax.ppermute(value, ('c', 'tp'), pairs)  22.6 us
    all_to_all x1, starting transfers between devices, layer(): lax.all_to_all(outgoing.reshape(depth, 2, capacity, cols_part), 'z', 0, 0...  15.7 us
    ppermute x7, waiting for transfers between devices, step(): return lax.ppermute(value, ('c', 'tp'), pairs)  11.8 us
    ppermute x1, starting transfers between devices, layer(): rows_other = lax.ppermute(arrived[:, 1], 'c', swap)  8.12 us
    all_to_all x1, waiting for transfers between devices, layer(): lax.all_to_all(outgoing.reshape(depth, 2, capacity, cols_part), 'z', 0, 0...  8.12 us
    ppermute x1, starting transfers between devices, layer(): lax.ppermute(returned[:, 1].reshape(half, cols_part), 'c', swap)  7.92 us
    all_to_all x2, starting transfers between devices, exchange(): lax.all_to_all(value, ('c', 'tp'), 0, 0, axis_index_groups=groups, tiled=...  7.83 us
  transfers between devices with their start and end apart: 14, of which 7 were waited for; matrix products, arithmetic and copies ran while one was open for 3% of the time, Pallas kernels for 3%

profile of v2, /device:TPU:1, one launch (start us, length us, event | category | flops | bytes accessed | tf_op | source)
XLA Modules:
  0.0 180.1 jit_solution(7971064026425691588)
XLA Ops:
  3.4 15.7 %all-to-all-start = ((bf16[16,2,32,128]{3,2,1,0:T(8,128)(2,1)}), bf16[16,2,32,128]{3,2,1,0:T(8,128)(2,1)S(1)}, u32[]{:S(2)}, u32[]{:S(2)}) async-start(bf16[16,2,32,128]{3,2,1,0:T(8,128)(2,1)} %bitcast.2), calls=%async_computation | async-start | bytes 524288 | tf_op jit(solution)/shard_map/all_to_all | solution.py:235
  20.3 4.4 %collective-permute-start.1 = (bf16[64,2]{1,0:T(8,128)(2,1)S(1)}, bf16[64,2]{1,0:T(8,128)(2,1)S(1)}, u32[]{:S(2)}, u32[]{:S(2)}) collective-permute-start(bf16[64,2]{1,0:T(8,128)(2,1)S(1)} %slice.54), channel_id=1, source_target_pairs={{0,16},{16,32},{32,48},{48,64},{64,80},{80,96},{96,112},{112,128},... | collective-permute-start | bytes 776 | tf_op jit(solution)/shard_map/ppermute | solution.py:245
  24.8 8.1 %all-to-all-done = bf16[16,2,32,128]{3,2,1,0:T(8,128)(2,1)S(1)} async-done(((bf16[16,2,32,128]{3,2,1,0:T(8,128)(2,1)}), bf16[16,2,32,128]{3,2,1,0:T(8,128)(2,1)S(1)}, u32[]{:S(2)}, u32[]{:S(2)}) %all-to-all-start) | async-done | bytes 262176 | tf_op jit(solution)/shard_map/all_to_all | solution.py:235
  32.9 8.1 %collective-permute-start = (bf16[16,32,128]{2,1,0:T(8,128)(2,1)S(1)}, bf16[16,32,128]{2,1,0:T(8,128)(2,1)S(1)}, u32[]{:S(2)}, u32[]{:S(2)}) collective-permute-start(bf16[16,32,128]{2,1,0:T(8,128)(2,1)S(1)} %get-tuple-element.31), channel_id=1, source_target_pairs={{0,16},{16,0},{1,17},{17,1},{2,18},{18,2},{3,19},{19,3},{4,20},{20... | collective-permute-start | bytes 393224 | tf_op jit(solution)/shard_map/ppermute | solution.py:284
  43.2 4.2 %all-to-all-start.1 = ((bf16[4,1024,128]{2,1,0:T(8,128)(2,1)}), bf16[4,1024,128]{2,1,0:T(8,128)(2,1)S(1)}, u32[]{:S(2)}, u32[]{:S(2)}) async-start(bf16[4,1024,128]{2,1,0:T(8,128)(2,1)} %broadcast_in_dim.14), calls=%async_computation.1 | async-start | bytes 2097152 | tf_op jit(solution)/shard_map/all_to_all | solution.py:280
  47.7 4.6 %collective-permute-start.2 = (bf16[2,32,2048]{2,1,0:T(8,128)(2,1)S(1)}, bf16[2,32,2048]{2,1,0:T(8,128)(2,1)S(1)}, u32[]{:S(2)}, u32[]{:S(2)}) collective-permute-start(bf16[2,32,2048]{2,1,0:T(8,128)(2,1)S(1)} %bitcast.39), channel_id=1, source_target_pairs={{0,3},{1,0},{2,1},{3,2},{4,7},{5,4},{6,5},{7,6},{8,11},{9,8},{10,9... | collective-permute-start | bytes 786440 | tf_op jit(solution)/shard_map/ppermute | solution.py:271
  52.3 2.5 %collective-permute-start.3 = (bf16[2,32,2048]{2,1,0:T(8,128)(2,1)S(1)}, bf16[2,32,2048]{2,1,0:T(8,128)(2,1)S(1)}, u32[]{:S(2)}, u32[]{:S(2)}) collective-permute-start(bf16[2,32,2048]{2,1,0:T(8,128)(2,1)S(1)} %bitcast.40), channel_id=1, source_target_pairs={{0,2},{1,3},{2,0},{3,1},{4,6},{5,7},{6,4},{7,5},{8,10},{9,11},{10,... | collective-permute-start | bytes 786440 | tf_op jit(solution)/shard_map/ppermute | solution.py:271
  54.8 2.5 %collective-permute-start.4 = (bf16[2,32,2048]{2,1,0:T(8,128)(2,1)S(1)}, bf16[2,32,2048]{2,1,0:T(8,128)(2,1)S(1)}, u32[]{:S(2)}, u32[]{:S(2)}) collective-permute-start(bf16[2,32,2048]{2,1,0:T(8,128)(2,1)S(1)} %bitcast.41), channel_id=1, source_target_pairs={{0,1},{1,2},{2,3},{3,0},{4,5},{5,6},{6,7},{7,4},{8,9},{9,10},{10,1... | collective-permute-start | bytes 786440 | tf_op jit(solution)/shard_map/ppermute | solution.py:271
  58.7 2.5 %collective-permute-done.3 = bf16[2,32,2048]{2,1,0:T(8,128)(2,1)S(1)} collective-permute-done((bf16[2,32,2048]{2,1,0:T(8,128)(2,1)S(1)}, bf16[2,32,2048]{2,1,0:T(8,128)(2,1)S(1)}, u32[]{:S(2)}, u32[]{:S(2)}) %collective-permute-start.3) | collective-permute-done | bytes 262176 | tf_op jit(solution)/shard_map/ppermute | solution.py:271
  61.2 2.8 %collective-permute-done.4 = bf16[2,32,2048]{2,1,0:T(8,128)(2,1)S(1)} collective-permute-done((bf16[2,32,2048]{2,1,0:T(8,128)(2,1)S(1)}, bf16[2,32,2048]{2,1,0:T(8,128)(2,1)S(1)}, u32[]{:S(2)}, u32[]{:S(2)}) %collective-permute-start.4) | collective-permute-done | bytes 262176 | tf_op jit(solution)/shard_map/ppermute | solution.py:271
  65.0 30.7 %all_to_all.30 = bf16[4,4,1024,128]{3,2,1,0:T(8,128)(2,1)S(1)} all-to-all(bf16[4,4,1024,128]{3,2,1,0:T(8,128)(2,1)S(1)} %broadcast_in_dim.15), channel_id=1, replica_groups={{0,4,8,12},{1,5,9,13},{2,6,10,14},{3,7,11,15},{16,17,18,19},{20,21,22,2..., dimensions={0} | all-to-all | bytes 8388608 | tf_op jit(solution)/shard_map/all_to_all | solution.py:280
  95.7 5.0 %shard_map.123 = bf16[16,1024,128]{2,1,0:T(8,128)(2,1)S(1)} custom-call(s32[1]{0:T(128)} %bitcast.me_ref, bf16[16,1024,128]{2,1,0:T(8,128)(2,1)S(1)} %bitcast.28, bf16[2048,256]{1,0:T(8,128)(2,1)S(1)} %bitcast.35, bf16[2048,256]{1,0:T(8,128)(2,1)S(1)} %bitcast.36, bf16[256,2048]{1,0:T(8,128)(2,1)S(1)} %bitcast.37), custom_call_target="tpu_custom_call" | custom-call | flops 3221225472 | bytes 11534336 | tf_op jit(solution)/shard_map/pallas_call | solution.py:100
  100.7 29.2 %all_to_all.31 = bf16[4,4,1024,128]{3,2,1,0:T(8,128)(2,1)S(1)} all-to-all(bf16[4,4,1024,128]{3,2,1,0:T(8,128)(2,1)S(1)} %bitcast.29), channel_id=1, replica_groups={{0,1,2,3},{4,5,6,7},{8,9,10,11},{12,13,14,15},{16,20,24,28},{17,21,25,2..., dimensions={0} | all-to-all | bytes 8388608 | tf_op jit(solution)/shard_map/all_to_all | solution.py:280
  131.5 3.6 %all-to-all-start.4 = ((bf16[4,1024,128]{2,1,0:T(8,128)(2,1)}), bf16[4,1024,128]{2,1,0:T(8,128)(2,1)S(1)}, u32[]{:S(2)}, u32[]{:S(2)}) async-start(bf16[4,1024,128]{2,1,0:T(8,128)(2,1)} %bitcast.16), calls=%async_computation.4 | async-start | bytes 2097152 | tf_op jit(solution)/shard_map/all_to_all | solution.py:280
  135.2 3.4 %collective-permute-start.6 = (bf16[8,32,2048]{2,1,0:T(8,128)(2,1)S(1)}, bf16[8,32,2048]{2,1,0:T(8,128)(2,1)S(1)}, u32[]{:S(2)}, u32[]{:S(2)}) collective-permute-start(bf16[8,32,2048]{2,1,0:T(8,128)(2,1)S(1)} %pad_maximum_fusion.refs_1_), channel_id=1, source_target_pairs={{0,4},{1,5},{2,6},{3,7},{4,8},{5,9},{6,10},{7,11},{8,12},{9,13},{1... | collective-permute-start | bytes 3145736 | tf_op jit(solution)/shard_map/ppermute | solution.py:271
  138.6 3.1 %collective-permute-start.5 = (bf16[8,32,2048]{2,1,0:T(8,128)(2,1)S(1)}, bf16[8,32,2048]{2,1,0:T(8,128)(2,1)}, u32[]{:S(2)}, u32[]{:S(2)}) collective-permute-start(bf16[8,32,2048]{2,1,0:T(8,128)(2,1)S(1)} %pad_maximum_fusion.refs_1_), channel_id=1, source_target_pairs={{0,12},{1,13},{2,14},{3,15},{4,0},{5,1},{6,2},{7,3},{8,4},{9,5},{1... | collective-permute-start | bytes 3145736 | tf_op jit(solution)/shard_map/ppermute | solution.py:271
  141.8 3.2 %all-to-all-done.4.in_ref = bf16[4,1024,128]{2,1,0:T(8,128)(2,1)S(1)} async-done(((bf16[4,1024,128]{2,1,0:T(8,128)(2,1)}), bf16[4,1024,128]{2,1,0:T(8,128)(2,1)S(1)}, u32[]{:S(2)}, u32[]{:S(2)}) %all-to-all-start.4) | async-done | bytes 1048608 | tf_op jit(solution)/shard_map/all_to_all | solution.py:280
  145.9 5.1 %all-to-all-start.5 = ((bf16[16,2,32,128]{3,2,1,0:T(8,128)(2,1)}), bf16[16,2,32,128]{3,2,1,0:T(8,128)(2,1)}, u32[]{:S(2)}, u32[]{:S(2)}) async-start(bf16[16,2,32,128]{3,2,1,0:T(8,128)(2,1)} %bitcast.32), calls=%async_computation.5 | async-start | bytes 524288 | tf_op jit(solution)/shard_map/all_to_all | solution.py:303
  151.0 5.1 %collective-permute-done.6.refs_3_ = bf16[8,32,2048]{2,1,0:T(8,128)(2,1)S(1)} collective-permute-done((bf16[8,32,2048]{2,1,0:T(8,128)(2,1)S(1)}, bf16[8,32,2048]{2,1,0:T(8,128)(2,1)S(1)}, u32[]{:S(2)}, u32[]{:S(2)}) %collective-permute-start.6) | collective-permute-done | bytes 1048608 | tf_op jit(solution)/shard_map/ppermute | solution.py:271
  156.9 1.9 %collective-permute-start.8 = (bf16[4,32,2048]{2,1,0:T(8,128)(2,1)}, bf16[4,32,2048]{2,1,0:T(8,128)(2,1)}, u32[]{:S(2)}, u32[]{:S(2)}) collective-permute-start(bf16[4,32,2048]{2,1,0:T(8,128)(2,1)} %slice.58), channel_id=1, source_target_pairs={{0,4},{1,5},{2,6},{3,7},{4,8},{5,9},{6,10},{7,11},{8,12},{9,13},{1... | collective-permute-start | bytes 1572872 | tf_op jit(solution)/shard_map/ppermute | solution.py:271
  160.7 4.6 %collective-permute-start.9 = (bf16[4,32,2048]{2,1,0:T(8,128)(2,1)}, bf16[4,32,2048]{2,1,0:T(8,128)(2,1)}, u32[]{:S(2)}, u32[]{:S(2)}) collective-permute-start(bf16[4,32,2048]{2,1,0:T(8,128)(2,1)} %slice.59), channel_id=1, source_target_pairs={{0,12},{1,13},{2,14},{3,15},{4,0},{5,1},{6,2},{7,3},{8,4},{9,5},{1... | collective-permute-start | bytes 1572872 | tf_op jit(solution)/shard_map/ppermute | solution.py:271
  165.3 2.1 %shard_map.126.refs_3_ = f32[128,2048]{1,0:T(8,128)S(1)} custom-call(s32[1]{0:T(128)} %bitcast.me_ref, bf16[16,64,128]{2,1,0:T(8,128)(2,1)S(1)} %bitcast.30, bf16[8,32,2048]{2,1,0:T(8,128)(2,1)S(1)} %pad_maximum_fusion.refs_1_, bf16[8,32,2048]{2,1,0:T(8,128)(2,1)} %collective-permute-done.5.refs_2_, bf16[8,32,2048]{2,1,0:T(8,128)(2,1)S(1)} %collective-permute-done.6.refs_3_), custom_call_target="tpu_custom_call" | custom-call | flops 402653184 | bytes 4456448 | tf_op jit(solution)/shard_map/pallas_call | solution.py:155
  168.4 7.9 %collective-permute-start.7 = (bf16[512,128]{1,0:T(8,128)(2,1)S(1)}, bf16[512,128]{1,0:T(8,128)(2,1)S(1)}, u32[]{:S(2)}, u32[]{:S(2)}) collective-permute-start(bf16[512,128]{1,0:T(8,128)(2,1)S(1)} %bitcast.43), channel_id=1, source_target_pairs={{0,16},{16,0},{1,17},{17,1},{2,18},{18,2},{3,19},{19,3},{4,20},{20... | collective-permute-start | bytes 393224 | tf_op jit(solution)/shard_map/ppermute | solution.py:310
  176.5 2.4 %shard_map.127 = bf16[2048,128]{1,0:T(8,128)(2,1)} custom-call(s32[1]{0:T(128)} %bitcast.me_ref, bf16[16,64,128]{2,1,0:T(8,128)(2,1)S(1)} %bitcast.31, bf16[4,32,2048]{2,1,0:T(8,128)(2,1)} %collective-permute-done.8.refs_1_, bf16[4,32,2048]{2,1,0:T(8,128)(2,1)} %collective-permute-done.9.refs_2_, f32[128,2048]{1,0:T(8,128)S(1)} %shard_map.126.refs_3_), custom_call_target="tpu_custom_call" | custom-call | flops 134217728 | bytes 2359296 | tf_op jit(solution)/shard_map/pallas_call | solution.py:155
  (48 shorter events, 16.5 us)
Async XLA Ops:
  0.6 24.1 %copy-start = (f32[3,1024]{1,0:T(4,128)S(1)}, f32[3,1024]{1,0:T(4,128)}, u32[]{:S(2)}) copy-start(f32[3,1024]{1,0:T(4,128)} %param.14) | copy-start | bytes 36868
  0.7 0.8 copy-start.3
  1.5 0.7 copy-start.4
  2.2 45.2 %copy-start.8 = (bf16[64,2048]{1,0:T(8,128)(2,1)S(1)}, bf16[64,2048]{1,0:T(8,128)(2,1)}, u32[]{:S(2)}) copy-start(bf16[64,2048]{1,0:T(8,128)(2,1)} %param.12) | copy-start | bytes 786436
  3.4 29.5 %all-to-all-start = ((bf16[16,2,32,128]{3,2,1,0:T(8,128)(2,1)}), bf16[16,2,32,128]{3,2,1,0:T(8,128)(2,1)S(1)}, u32[]{:S(2)}, u32[]{:S(2)}) async-start(bf16[16,2,32,128]{3,2,1,0:T(8,128)(2,1)} %bitcast.2), calls=%async_computation | async-start | bytes 524288 | tf_op jit(solution)/shard_map/all_to_all | solution.py:235
  20.3 20.8 %collective-permute-start.1 = (bf16[64,2]{1,0:T(8,128)(2,1)S(1)}, bf16[64,2]{1,0:T(8,128)(2,1)S(1)}, u32[]{:S(2)}, u32[]{:S(2)}) collective-permute-start(bf16[64,2]{1,0:T(8,128)(2,1)S(1)} %slice.54), channel_id=1, source_target_pairs={{0,16},{16,32},{32,48},{48,64},{64,80},{80,96},{96,112},{112,128},... | collective-permute-start | bytes 776 | tf_op jit(solution)/shard_map/ppermute | solution.py:245
  32.9 9.1 %collective-permute-start = (bf16[16,32,128]{2,1,0:T(8,128)(2,1)S(1)}, bf16[16,32,128]{2,1,0:T(8,128)(2,1)S(1)}, u32[]{:S(2)}, u32[]{:S(2)}) collective-permute-start(bf16[16,32,128]{2,1,0:T(8,128)(2,1)S(1)} %get-tuple-element.31), channel_id=1, source_target_pairs={{0,16},{16,0},{1,17},{17,1},{2,18},{18,2},{3,19},{19,3},{4,20},{20... | collective-permute-start | bytes 393224 | tf_op jit(solution)/shard_map/ppermute | solution.py:284
  43.2 21.0 %all-to-all-start.1 = ((bf16[4,1024,128]{2,1,0:T(8,128)(2,1)}), bf16[4,1024,128]{2,1,0:T(8,128)(2,1)S(1)}, u32[]{:S(2)}, u32[]{:S(2)}) async-start(bf16[4,1024,128]{2,1,0:T(8,128)(2,1)} %broadcast_in_dim.14), calls=%async_computation.1 | async-start | bytes 2097152 | tf_op jit(solution)/shard_map/all_to_all | solution.py:280
  47.7 11.0 %collective-permute-start.2 = (bf16[2,32,2048]{2,1,0:T(8,128)(2,1)S(1)}, bf16[2,32,2048]{2,1,0:T(8,128)(2,1)S(1)}, u32[]{:S(2)}, u32[]{:S(2)}) collective-permute-start(bf16[2,32,2048]{2,1,0:T(8,128)(2,1)S(1)} %bitcast.39), channel_id=1, source_target_pairs={{0,3},{1,0},{2,1},{3,2},{4,7},{5,4},{6,5},{7,6},{8,11},{9,8},{10,9... | collective-permute-start | bytes 786440 | tf_op jit(solution)/shard_map/ppermute | solution.py:271
  52.3 8.9 %collective-permute-start.3 = (bf16[2,32,2048]{2,1,0:T(8,128)(2,1)S(1)}, bf16[2,32,2048]{2,1,0:T(8,128)(2,1)S(1)}, u32[]{:S(2)}, u32[]{:S(2)}) collective-permute-start(bf16[2,32,2048]{2,1,0:T(8,128)(2,1)S(1)} %bitcast.40), channel_id=1, source_target_pairs={{0,2},{1,3},{2,0},{3,1},{4,6},{5,7},{6,4},{7,5},{8,10},{9,11},{10,... | collective-permute-start | bytes 786440 | tf_op jit(solution)/shard_map/ppermute | solution.py:271
  54.8 9.2 %collective-permute-start.4 = (bf16[2,32,2048]{2,1,0:T(8,128)(2,1)S(1)}, bf16[2,32,2048]{2,1,0:T(8,128)(2,1)S(1)}, u32[]{:S(2)}, u32[]{:S(2)}) collective-permute-start(bf16[2,32,2048]{2,1,0:T(8,128)(2,1)S(1)} %bitcast.41), channel_id=1, source_target_pairs={{0,1},{1,2},{2,3},{3,0},{4,5},{5,6},{6,7},{7,4},{8,9},{9,10},{10,1... | collective-permute-start | bytes 786440 | tf_op jit(solution)/shard_map/ppermute | solution.py:271
  65.0 30.7 %copy-start.5 = (bf16[1,2048,256]{2,1,0:T(8,128)(2,1)S(1)}, bf16[1,2048,256]{2,1,0:T(8,128)(2,1)}, u32[]{:S(2)}) copy-start(bf16[1,2048,256]{2,1,0:T(8,128)(2,1)} %param.19) | copy-start | bytes 3145732
  65.0 30.7 %copy-start.6 = (bf16[1,2048,256]{2,1,0:T(8,128)(2,1)S(1)}, bf16[1,2048,256]{2,1,0:T(8,128)(2,1)}, u32[]{:S(2)}) copy-start(bf16[1,2048,256]{2,1,0:T(8,128)(2,1)} %param.20) | copy-start | bytes 3145732
  65.0 30.7 %copy-start.7 = (bf16[1,256,2048]{2,1,0:T(8,128)(2,1)S(1)}, bf16[1,256,2048]{2,1,0:T(8,128)(2,1)}, u32[]{:S(2)}) copy-start(bf16[1,256,2048]{2,1,0:T(8,128)(2,1)} %param.21) | copy-start | bytes 3145732
  131.5 33.8 %copy-start.1 = (bf16[1024,128]{1,0:T(8,128)(2,1)S(1)}, bf16[1024,128]{1,0:T(8,128)(2,1)}, u32[]{:S(2)}) copy-start(bf16[1024,128]{1,0:T(8,128)(2,1)} %param.15) | copy-start | bytes 786436
  131.5 13.5 %all-to-all-start.4 = ((bf16[4,1024,128]{2,1,0:T(8,128)(2,1)}), bf16[4,1024,128]{2,1,0:T(8,128)(2,1)S(1)}, u32[]{:S(2)}, u32[]{:S(2)}) async-start(bf16[4,1024,128]{2,1,0:T(8,128)(2,1)} %bitcast.16), calls=%async_computation.4 | async-start | bytes 2097152 | tf_op jit(solution)/shard_map/all_to_all | solution.py:280
  135.1 41.2 %copy-start.9 = (f32[256,2]{0,1:T(2,128)S(1)}, f32[256,2]{0,1:T(2,128)}, u32[]{:S(2)}) copy-start(f32[256,2]{0,1:T(2,128)} %param.18) | copy-start | bytes 6148
  135.2 20.9 %collective-permute-start.6 = (bf16[8,32,2048]{2,1,0:T(8,128)(2,1)S(1)}, bf16[8,32,2048]{2,1,0:T(8,128)(2,1)S(1)}, u32[]{:S(2)}, u32[]{:S(2)}) collective-permute-start(bf16[8,32,2048]{2,1,0:T(8,128)(2,1)S(1)} %pad_maximum_fusion.refs_1_), channel_id=1, source_target_pairs={{0,4},{1,5},{2,6},{3,7},{4,8},{5,9},{6,10},{7,11},{8,12},{9,13},{1... | collective-permute-start | bytes 3145736 | tf_op jit(solution)/shard_map/ppermute | solution.py:271
  138.6 20.2 %collective-permute-start.5 = (bf16[8,32,2048]{2,1,0:T(8,128)(2,1)S(1)}, bf16[8,32,2048]{2,1,0:T(8,128)(2,1)}, u32[]{:S(2)}, u32[]{:S(2)}) collective-permute-start(bf16[8,32,2048]{2,1,0:T(8,128)(2,1)S(1)} %pad_maximum_fusion.refs_1_), channel_id=1, source_target_pairs={{0,12},{1,13},{2,14},{3,15},{4,0},{5,1},{6,2},{7,3},{8,4},{9,5},{1... | collective-permute-start | bytes 3145736 | tf_op jit(solution)/shard_map/ppermute | solution.py:271
  145.2 0.7 copy-start.2
  145.9 21.5 %all-to-all-start.5 = ((bf16[16,2,32,128]{3,2,1,0:T(8,128)(2,1)}), bf16[16,2,32,128]{3,2,1,0:T(8,128)(2,1)}, u32[]{:S(2)}, u32[]{:S(2)}) async-start(bf16[16,2,32,128]{3,2,1,0:T(8,128)(2,1)} %bitcast.32), calls=%async_computation.5 | async-start | bytes 524288 | tf_op jit(solution)/shard_map/all_to_all | solution.py:303
  156.9 19.6 %collective-permute-start.8 = (bf16[4,32,2048]{2,1,0:T(8,128)(2,1)}, bf16[4,32,2048]{2,1,0:T(8,128)(2,1)}, u32[]{:S(2)}, u32[]{:S(2)}) collective-permute-start(bf16[4,32,2048]{2,1,0:T(8,128)(2,1)} %slice.58), channel_id=1, source_target_pairs={{0,4},{1,5},{2,6},{3,7},{4,8},{5,9},{6,10},{7,11},{8,12},{9,13},{1... | collective-permute-start | bytes 1572872 | tf_op jit(solution)/shard_map/ppermute | solution.py:271
  160.7 15.8 %collective-permute-start.9 = (bf16[4,32,2048]{2,1,0:T(8,128)(2,1)}, bf16[4,32,2048]{2,1,0:T(8,128)(2,1)}, u32[]{:S(2)}, u32[]{:S(2)}) collective-permute-start(bf16[4,32,2048]{2,1,0:T(8,128)(2,1)} %slice.59), channel_id=1, source_target_pairs={{0,12},{1,13},{2,14},{3,15},{4,0},{5,1},{6,2},{7,3},{8,4},{9,5},{1... | collective-permute-start | bytes 1572872 | tf_op jit(solution)/shard_map/ppermute | solution.py:271
  168.4 10.5 %collective-permute-start.7 = (bf16[512,128]{1,0:T(8,128)(2,1)S(1)}, bf16[512,128]{1,0:T(8,128)(2,1)S(1)}, u32[]{:S(2)}, u32[]{:S(2)}) collective-permute-start(bf16[512,128]{1,0:T(8,128)(2,1)S(1)} %bitcast.43), channel_id=1, source_target_pairs={{0,16},{16,0},{1,17},{17,1},{2,18},{18,2},{3,19},{19,3},{4,20},{20... | collective-permute-start | bytes 393224 | tf_op jit(solution)/shard_map/ppermute | solution.py:310
